TPU v7x, 512 devices: a whole 4x8x8 slice. The times are simulated.
512 devices in a mesh: sp: 64 (over z, y), tp: 8 (over x, core).
Axes of the slice: x: 4, y: 8, z: 8, core: 2. Of those that a mesh axis runs over, the one named last changes fastest.
Arguments:
- residual: bfloat16 [8192, 2048], P(('sp', 'tp')), may hold values from -6 to 6
- q_small: bfloat16 [8192, 1024], P('sp', 'tp'), may hold values from -6 to 6
- k_small: bfloat16 [8192, 1024], P('sp', 'tp'), may hold values from -6 to 6
- v_small: bfloat16 [8192, 1024], P('sp', 'tp'), may hold values from -6 to 6
- q_large: bfloat16 [8192, 1024], P('sp', 'tp'), may hold values from -6 to 6
- k_large: bfloat16 [8192, 1024], P('sp', 'tp'), may hold values from -6 to 6
- v_large: bfloat16 [8192, 1024], P('sp', 'tp'), may hold values from -6 to 6
- forget_small: float32 [8192, 16], P('sp', 'tp'), may hold values from 0 to 20
- forget_large: float32 [8192, 8], P('sp', 'tp'), may hold values from 0 to 20
- w_out_small: bfloat16 [1024, 2048], P('tp'), may hold values from -0.125 to 0.125
- w_out_large: bfloat16 [1024, 2048], P('tp'), may hold values from -0.125 to 0.125
- norm_gain: float32 [2048], replicated, may hold values from 0.1 to 1.9
- w_gate: bfloat16 [2048, 4096], P('sp', 'tp'), may hold values from -0.125 to 0.125
- w_up: bfloat16 [2048, 4096], P('sp', 'tp'), may hold values from -0.125 to 0.125
- conv_gate: float32 [3, 4096], P(None, 'tp'), may hold values from -3 to 3
- conv_up: float32 [3, 4096], P(None, 'tp'), may hold values from -3 to 3
- w_down: bfloat16 [4096, 2048], P('tp', 'sp'), may hold values from -0.09375 to 0.09375
Outputs:
- mixed: bfloat16 [8192, 2048], P(('sp', 'tp'))
All inputs are finite; a program needn't handle non-finite values.
Results may differ from a plain program's by a relative error of at most 0.015.
Values may be sent and summed in bfloat16 or wider, within the bound.
A program may use at most 64 MiB of HBM per device.

v0:
```python
import jax
import jax.numpy as jnp
from jax import lax
from jax.sharding import PartitionSpec as P

EPS = 1e-06
NEG = -1e30


def rows_first(arrays, axis, dims):
    turned = [jnp.moveaxis(a, dim, 0) for a, dim in zip(arrays, dims)]
    widths = [t[0].size for t in turned]
    both = jnp.concatenate([t.reshape(-1, w) for t, w in zip(turned, widths)], axis=1)
    whole = lax.all_gather(both, axis, axis=0, tiled=True)
    parts = jnp.split(whole, [sum(widths[:k]) for k in range(1, len(widths))], axis=1)
    return tuple(
        (
            jnp.moveaxis(b.reshape(-1, *t.shape[1:]), 0, dim)
            for b, t, dim in zip(parts, turned, dims)
        )
    )


def in_one_piece(arrays, axis, dim, along):
    widths = [a.shape[along] for a in arrays]
    both = jnp.concatenate(arrays, axis=along)
    whole = lax.all_gather(both, axis, axis=dim, tiled=True)
    return tuple(jnp.split(whole, [sum(widths[:k]) for k in range(1, len(widths))], axis=along))


def in_blocks(array, dim, size):
    before, after = (array.shape[:dim], array.shape[dim + 1 :])
    return jnp.moveaxis(array.reshape(*before, size, -1, *after), dim, 0)


def sent_and_summed(array, axis, dim):
    size = lax.axis_size(axis)
    parts = lax.all_to_all(in_blocks(array, dim, size), axis, 0, 0, tiled=True)
    return jnp.sum(parts.astype(jnp.float32), axis=0)


def sent_to_all(array, axis):
    size = lax.axis_size(axis)
    return lax.all_to_all(
        jnp.broadcast_to(array[None], (size, *array.shape)), axis, 0, 0, tiled=True
    )


def in_order(parts, dim):
    parts = jnp.moveaxis(parts, 0, dim)
    lengths = parts.shape
    return parts.reshape(*lengths[:dim], lengths[dim] * lengths[dim + 1], *lengths[dim + 2 :])


def gather_directly(array, axis, dim):
    parts = sent_to_all(array, axis)
    return in_order(parts, dim)


def from_behind(block, axis, distance):
    devices = range(lax.axis_size(axis))
    route = [(i - distance, i) for i in devices if i - distance in devices]
    return lax.ppermute(block, axis, route)


def globalize(part, rows):
    heads = part.shape[1]
    blocks = part.reshape(-1, rows, heads)
    totals = blocks[:, -1, :]
    before = jnp.cumsum(totals, axis=0) - totals
    return (blocks + before[:, None, :]).reshape(part.shape)


def attend(carry, keys, values, queries, cum_own, cum_every, qpos):
    top, denom, accum = carry
    count = keys.shape[0]
    heads = queries.shape[1]
    size = queries.shape[2]
    keys = keys.reshape(count, heads, size)
    values = values.reshape(count, heads, size)
    kpos = jnp.arange(count, dtype=jnp.int32)
    scores = jnp.einsum(
        "qhd,khd->qhk", queries, keys, preferred_element_type=jnp.float32
    ) * size ** (-0.5)
    scores = scores + cum_own[:, :, None] - cum_every.T[None, :, :]
    keep = (kpos[None, :] <= qpos[:, None])[:, None, :]
    scores = jnp.where(keep, scores, NEG)
    new_top = jnp.maximum(top, jnp.max(scores, axis=-1))
    weights = jnp.where(keep, jnp.exp(scores - new_top[:, :, None]), 0.0)
    denom = jnp.sum(weights, axis=-1)
    accum = jnp.einsum(
        "qhk,khd->qhd", weights.astype(jnp.bfloat16), values, preferred_element_type=jnp.float32
    )
    return (new_top, denom, accum)


def finish(carry):
    top, denom, accum = carry
    attended = accum / denom[:, :, None]
    normed = attended * lax.rsqrt(jnp.mean(attended * attended, axis=-1, keepdims=True) + EPS)
    return normed.astype(jnp.bfloat16).reshape(attended.shape[0], -1)


def empty_carry(rows, heads, size):
    return (
        jnp.full((rows, heads), NEG, jnp.float32),
        jnp.zeros((rows, heads), jnp.float32),
        jnp.zeros((rows, heads, size), jnp.float32),
    )


def body(
    residual,
    q_small,
    k_small,
    v_small,
    q_large,
    k_large,
    v_large,
    forget_small,
    forget_large,
    w_out_small,
    w_out_large,
    norm_gain,
    w_gate,
    w_up,
    conv_gate,
    conv_up,
    w_down,
):
    rows = q_small.shape[0]
    offset = lax.axis_index("sp") * rows
    qpos = offset + jnp.arange(rows, dtype=jnp.int32)
    gathered = rows_first((w_gate, w_up, w_down), "sp", (0, 0, 1))
    local_small = jnp.cumsum(jax.nn.log_sigmoid(forget_small), axis=0)
    local_large = jnp.cumsum(jax.nn.log_sigmoid(forget_large), axis=0)
    part_small, part_large = in_one_piece((local_small, local_large), "sp", 0, 1)
    every_small = globalize(part_small, rows)
    every_large = globalize(part_large, rows)
    cum_small = lax.dynamic_slice_in_dim(every_small, offset, rows, 0)
    cum_large = lax.dynamic_slice_in_dim(every_large, offset, rows, 0)
    heads_small = forget_small.shape[1]
    heads_large = forget_large.shape[1]
    queries_small = q_small.reshape(rows, heads_small, -1)
    queries_large = q_large.reshape(rows, heads_large, -1)
    start_carry = (
        empty_carry(rows, heads_small, queries_small.shape[2]),
        empty_carry(rows, heads_large, queries_large.shape[2]),
    )
    keys_s, values_s, keys_l, values_l = in_one_piece(
        (k_small, v_small, k_large, v_large), "sp", 0, 1
    )
    small = attend(start_carry[0], keys_s, values_s, queries_small, cum_small, every_small, qpos)
    large = attend(start_carry[1], keys_l, values_l, queries_large, cum_large, every_large, qpos)
    normed_small = finish(small)
    normed_large = finish(large)
    first_part = jnp.dot(normed_small, w_out_small, preferred_element_type=jnp.float32)
    projected = sent_and_summed(
        (
            first_part + jnp.dot(normed_large, w_out_large, preferred_element_type=jnp.float32)
        ).astype(jnp.bfloat16),
        "tp",
        0,
    )
    first = residual.astype(jnp.float32) + projected
    normal = (
        first * lax.rsqrt(jnp.mean(first * first, axis=-1, keepdims=True) + EPS) * norm_gain
    ).astype(jnp.bfloat16)
    gate_full, up_full, down_full = gathered
    piece = gather_directly(normal, "tp", 0)
    gate_part = jnp.dot(piece, gate_full, preferred_element_type=jnp.float32).astype(jnp.bfloat16)
    up_part = jnp.dot(piece, up_full, preferred_element_type=jnp.float32).astype(jnp.bfloat16)
    both = jnp.concatenate([gate_part, up_part], axis=1)
    width = both.shape[0]
    rim = from_behind(both[width - 2 :], "sp", 1)
    extended = jnp.concatenate([rim, both], axis=0).astype(jnp.float32)
    taps = jnp.concatenate([conv_gate, conv_up], axis=1)
    conv = (
        taps[0] * extended[0:width]
        + taps[1] * extended[1 : width + 1]
        + taps[2] * extended[2 : width + 2]
    )
    half = gate_full.shape[1]
    hidden = (jax.nn.silu(conv[:, :half]) * conv[:, half:]).astype(jnp.bfloat16)
    mixed = first + sent_and_summed(
        jnp.dot(hidden, down_full, preferred_element_type=jnp.float32).astype(jnp.bfloat16), "tp", 0
    )
    return mixed.astype(jnp.bfloat16)


def solution(mesh):
    placed = (
        P(("sp", "tp"), None),
        P("sp", "tp"),
        P("sp", "tp"),
        P("sp", "tp"),
        P("sp", "tp"),
        P("sp", "tp"),
        P("sp", "tp"),
        P("sp", "tp"),
        P("sp", "tp"),
        P("tp", None),
        P("tp", None),
        P(),
        P("sp", "tp"),
        P("sp", "tp"),
        P(None, "tp"),
        P(None, "tp"),
        P("tp", "sp"),
    )
    return jax.shard_map(
        body, mesh=mesh, in_specs=placed, out_specs=P(("sp", "tp"), None), check_vma=False
    )
```

profile of v0, /device:TPU:1, one launch (start us, length us, event | category | flops | bytes accessed | tf_op | source)
XLA Modules:
  0.0 239.2 jit_solution(16217018536142575278)
XLA Ops:
  6.5 1.5 pad_maximum_fusion
  8.2 1.4 pad_maximum_fusion.1
  11.7 47.5 %all_gather.10 = f32[8192,3]{0,1:T(4,128)S(1)} all-gather(f32[128,3]{0,1:T(4,128)S(1)} %pad_maximum_fusion.3), channel_id=1, replica_groups=mesh['sp'=64,'tp'=8] {'sp'}, dimensions={0}, use_global_device_ids=true | all-gather | bytes 99840 | tf_op jit(solution)/shard_map/all_gather | solution.py:27
  60.0 2.7 %copy.48 = f32[8192,2]{1,0:T(8,128)} copy(f32[8192,2]{0,1:T(2,128)S(1)} %split.38) | data formatting | bytes 131072 | tf_op jit(solution)/shard_map/split | solution.py:28
  62.7 1.3 reduce-window_subtract_fusion.1
  64.5 1.7 iota_compare_fusion.1
  66.2 48.6 %all-gather.3.cloned.1.call-done = bf16[8192,512]{1,0:T(8,128)(2,1)} async-done(((bf16[128,512]{1,0:T(8,128)(2,1)}), bf16[8192,512]{1,0:T(8,128)(2,1)}) %all-gather.3.cloned.1.call-update) | async-done | bytes 8388624 | tf_op jit(solution)/shard_map/all_gather | solution.py:27
  114.8 3.9 %fusion.70 = (bf16[8192,128]{1,0:T(8,128)(2,1)}, bf16[8192,128]{1,0:T(8,128)(2,1)S(1)}) fusion(bf16[8192,512]{1,0:T(8,128)(2,1)} %all-gather.3.cloned.1.call-done), kind=kLoop, calls=%fused_computation.95 | loop fusion | bytes 8388608 | tf_op jit(solution)/shard_map/split | solution.py:28
  118.7 4.1 %copy.42 = bf16[8192,128]{0,1:T(8,128)(2,1)} copy(bf16[8192,128]{1,0:T(8,128)(2,1)} %get-tuple-element.5) | data formatting | bytes 4194304 | tf_op jit(solution)/shard_map/split | solution.py:28
  122.8 2.9 %copy.41 = bf16[8192,128]{0,1:T(8,128)(2,1)} copy(bf16[8192,128]{1,0:T(8,128)(2,1)S(1)} %get-tuple-element.6) | data formatting | bytes 4194304 | tf_op jit(solution)/shard_map/split | solution.py:28
  125.7 3.5 %fusion.74 = (f32[128]{0:T(128)S(1)}, f32[128,1,8192]{0,2,1:T(8,128)S(1)}) fusion(f32[8192]{0:T(1024)S(1)} %bitcast_add_fusion.1, f32[128]{0:T(128)S(1)} %fusion.65, bf16[128,128]{1,0:T(8,128)(2,1)S(1)} %copy-done.10, bf16[8192,512]{1,0:T(8,128)(2,1)} %all-gather.3.cloned.1.call-done, s32[128]{0:T(128)S(1)} %iota_add_fusion), kind=kOutput, calls=%fused_computation.99 | convolution fusion | flops 274726784 | bytes 6358528 | tf_op jit(solution)/shard_map/qhd,khd->qhk/dot_general | solution.py:82
  129.2 1.1 fusion.16
  130.4 3.0 %multiply_reduce_fusion.1 = (f32[128]{0:T(128)S(1)}, f32[1,128,128]{2,1,0:T(8,128)S(1)}) fusion(f32[128]{0:T(128)S(1)} %fusion.16, f32[128,1,8192]{0,2,1:T(8,128)S(1)} %get-tuple-element.15, f32[128]{0:T(128)S(1)} %broadcast_maximum_fusion.1, s32[128]{0:T(128)S(1)} %iota_add_fusion, bf16[8192,512]{1,0:T(8,128)(2,1)} %all-gather.3.cloned.1.call-done), kind=kOutput, calls=%fused_computation.65 | convolution fusion | flops 272678784 | bytes 6359040 | tf_op jit(solution)/shard_map/qhk,khd->qhd/dot_general | solution.py:91
  133.4 3.6 %fusion.72 = (f32[128,2]{0,1:T(2,128)S(1)}, f32[128,2,8192]{0,2,1:T(8,128)S(1)}) fusion(f32[2,8192]{1,0:T(2,128)S(1)} %bitcast.93, f32[128,2]{0,1:T(2,128)S(1)} %constant_dynamic-slice_fusion.2, bf16[8192,2,64]{0,2,1:T(8,128)(2,1)S(1)} %bitcast.85, bf16[128,2,64]{0,2,1:T(8,128)(2,1)S(1)} %bitcast.95, pred[128,8192]{0,1:T(8,128)(4,1)S(1)} %copy-done.1), kind=kOutput, calls=%fused_computation.97 | convolution fusion | flops 278920960 | bytes 11634688 | tf_op jit(solution)/shard_map/qhd,khd->qhk/dot_general | solution.py:82
  137.0 1.7 fusion.9
  138.7 2.1 multiply_reduce_fusion.2
  141.6 14.3 %all_to_all.15 = bf16[8,16,2048]{2,1,0:T(8,128)(2,1)S(1)} all-to-all(bf16[8,16,2048]{2,1,0:T(8,128)(2,1)S(1)} %bitcast.83), channel_id=1, replica_groups=mesh['sp'=64,'tp'=8] {'tp'}, dimensions={0} | all-to-all | bytes 1048576 | tf_op jit(solution)/shard_map/all_to_all | solution.py:38
  157.1 4.4 %all-to-all-start.1 = ((bf16[8,16,2048]{2,1,0:T(8,128)(2,1)}), bf16[8,16,2048]{2,1,0:T(8,128)(2,1)S(1)}, u32[]{:S(2)}, u32[]{:S(2)}) async-start(bf16[8,16,2048]{2,1,0:T(8,128)(2,1)} %broadcast_in_dim.63), calls=%async_computation.1 | async-start | bytes 1048576 | tf_op jit(solution)/shard_map/all_to_all | solution.py:44
  161.5 43.9 %all-gather.5.cloned.1.call-done = bf16[2048,1536]{1,0:T(8,128)(2,1)} async-done(((bf16[32,1536]{1,0:T(8,128)(2,1)}), bf16[2048,1536]{1,0:T(8,128)(2,1)}) %all-gather.5.cloned.1.call-update) | async-done | bytes 6291472 | tf_op jit(solution)/shard_map/all_gather | solution.py:14
  205.5 2.0 fusion.32
  207.5 2.0 fusion.35
  209.6 1.9 collective-permute-start
  212.5 2.4 %convolution_convert_fusion = bf16[128,2048]{1,0:T(8,128)(2,1)S(1)} fusion(bf16[2048,1536]{1,0:T(8,128)(2,1)} %all-gather.5.cloned.1.call-done, f32[128,1024]{1,0:T(8,128)S(1)} %fusion.54), kind=kOutput, calls=%fused_computation.25 | convolution fusion | flops 269090816 | bytes 3145728 | tf_op jit(solution)/shard_map/dot_general | solution.py:186
  214.9 16.7 %all_to_all.16 = bf16[8,16,2048]{2,1,0:T(8,128)(2,1)S(1)} all-to-all(bf16[8,16,2048]{2,1,0:T(8,128)(2,1)S(1)} %bitcast.88), channel_id=1, replica_groups=mesh['sp'=64,'tp'=8] {'tp'}, dimensions={0} | all-to-all | bytes 1048576 | tf_op jit(solution)/shard_map/all_to_all | solution.py:38
  (70 shorter events, 7.0 us)
Async XLA Ops:
  6.5 134.4 %copy-start = (bf16[128,2048]{1,0:T(8,128)(2,1)S(1)}, bf16[128,2048]{1,0:T(8,128)(2,1)}, u32[]{:S(2)}) copy-start(bf16[128,2048]{1,0:T(8,128)(2,1)} %param.26) | copy-start | bytes 1572868
  6.5 57.6 %copy-start.6 = (bf16[128,128]{1,0:T(8,128)(2,1)S(1)}, bf16[128,128]{1,0:T(8,128)(2,1)}, u32[]{:S(2)}) copy-start(bf16[128,128]{1,0:T(8,128)(2,1)} %param.18) | copy-start | bytes 98308
  6.5 108.3 %all-gather.3.cloned.1.call-start = ((), (), s32[]{:S(2)}) async-start(), calls=%async_computation.3 | async-start | bytes 8519680 | tf_op jit(solution)/shard_map/all_gather | solution.py:27
  8.1 197.4 %all-gather.5.cloned.1.call-start = ((), (), s32[]{:S(2)}) async-start(), calls=%async_computation.4 | async-start | bytes 6389760 | tf_op jit(solution)/shard_map/all_gather | solution.py:14
  118.7 7.0 %copy-start.10 = (bf16[128,128]{1,0:T(8,128)(2,1)S(1)}, bf16[128,128]{1,0:T(8,128)(2,1)}, u32[]{:S(2)}) copy-start(bf16[128,128]{1,0:T(8,128)(2,1)} %param.21) | copy-start | bytes 98308
  130.3 3.0 %copy-start.1 = (pred[128,8192]{0,1:T(8,128)(4,1)S(1)}, pred[128,8192]{0,1:T(8,128)(4,1)}, u32[]{:S(2)}) copy-start(pred[128,8192]{0,1:T(8,128)(4,1)} %iota_compare_fusion.1) | copy-start | bytes 3145732
  130.3 3.0 %copy-start.3 = (bf16[8192,128]{0,1:T(8,128)(2,1)S(1)}, bf16[8192,128]{0,1:T(8,128)(2,1)}, u32[]{:S(2)}) copy-start(bf16[8192,128]{0,1:T(8,128)(2,1)} %copy.42) | copy-start | bytes 6291460
  137.0 1.7 copy-start.2
  138.7 2.6 %copy-start.5 = (bf16[128,2048]{1,0:T(8,128)(2,1)S(1)}, bf16[128,2048]{1,0:T(8,128)(2,1)}, u32[]{:S(2)}) copy-start(bf16[128,2048]{1,0:T(8,128)(2,1)} %param.27) | copy-start | bytes 1572868
  140.9 15.1 %copy-start.4 = (bf16[16,2048]{1,0:T(8,128)(2,1)S(1)}, bf16[16,2048]{1,0:T(8,128)(2,1)}, u32[]{:S(2)}) copy-start(bf16[16,2048]{1,0:T(8,128)(2,1)} %param.17) | copy-start | bytes 196612
  140.9 15.3 %copy-start.7 = (f32[2048]{0:T(1024)S(1)}, f32[2048]{0:T(1024)}, u32[]{:S(2)}) copy-start(f32[2048]{0:T(1024)} %param.28) | copy-start | bytes 24580
  140.9 20.6 %copy-start.8 = (f32[3,512]{1,0:T(4,128)S(1)}, f32[3,512]{1,0:T(4,128)}, u32[]{:S(2)}) copy-start(f32[3,512]{1,0:T(4,128)} %param.31) | copy-start | bytes 18436
  140.9 20.6 %copy-start.9 = (f32[3,512]{1,0:T(4,128)S(1)}, f32[3,512]{1,0:T(4,128)}, u32[]{:S(2)}) copy-start(f32[3,512]{1,0:T(4,128)} %param.32) | copy-start | bytes 18436
  157.1 48.4 %all-to-all-start.1 = ((bf16[8,16,2048]{2,1,0:T(8,128)(2,1)}), bf16[8,16,2048]{2,1,0:T(8,128)(2,1)S(1)}, u32[]{:S(2)}, u32[]{:S(2)}) async-start(bf16[8,16,2048]{2,1,0:T(8,128)(2,1)} %broadcast_in_dim.63), calls=%async_computation.1 | async-start | bytes 1048576 | tf_op jit(solution)/shard_map/all_to_all | solution.py:44
  209.6 2.6 %collective-permute-start = (bf16[2,1024]{1,0:T(2,128)(2,1)S(1)}, bf16[2,1024]{1,0:T(2,128)(2,1)S(1)}, u32[]{:S(2)}, u32[]{:S(2)}) collective-permute-start(bf16[2,1024]{1,0:T(2,128)(2,1)S(1)} %pad_maximum_fusion.2), channel_id=1, source_target_pairs={{0,8},{8,16},{16,24},{24,32},{32,40},{40,48},{48,56},{56,64},{64,7... | collective-permute-start | bytes 12296 | tf_op jit(solution)/shard_map/ppermute | solution.py:63
Sparse Core Ops, SparseCore 0:
  10.4 104.3 all-gather.2
  117.8 87.6 all-gather.4
where the time goes:
time: 241 us; the launch traced here: 239 us
  waiting for transfers between devices  93.3 us (39%)
  blocking collectives  78.5 us (33%)
  matrix products  19.4 us (8%)
  local copies, waits for them, and re-layouts  15.3 us (6%)
  between operations  13.7 us (6%)
  other arithmetic  12.5 us (5%)
  starting transfers between devices  6.38 us (3%)
    all_gather x1, waiting for transfers between devices, in_one_piece(): whole = lax.all_gather(both, axis, axis=dim, tiled=True)  48.6 us
    all_gather x1, blocking collectives, in_one_piece(): whole = lax.all_gather(both, axis, axis=dim, tiled=True)  47.5 us
    all_gather x1, waiting for transfers between devices, rows_first(): whole = lax.all_gather(both, axis, axis=0, tiled=True)  43.9 us
    all_to_all x2, blocking collectives, sent_and_summed(): parts = lax.all_to_all(in_blocks(array, dim, size), axis, 0, 0, tiled=True)  31 us
    split x6, local copies, waits for them, and re-layouts, in_one_piece(): jnp.split(whole, [sum(widths[:k]) for k in range(1, len(widths))], axis=a...  13.6 us
    dot_general x2, matrix products, attend(): jnp.einsum('qhd,khd->qhk', queries, keys, preferred_element_type=jnp.floa...  7.16 us
    dot_general x2, matrix products, attend(): jnp.einsum('qhk,khd->qhd', weights.astype(jnp.bfloat16), values, preferre...  5.11 us
  transfers between devices with their start and end apart: 4, of which 3 were waited for; matrix products, arithmetic and copies ran while one was open for 16% of the time, Pallas kernels for 0%

commit v1 on v0

v1 whole, which is shorter than its diff:
```python
import functools
import math

import jax
import jax.numpy as jnp
from jax import lax
from jax.experimental import pallas as pl
from jax.experimental.pallas import tpu as pltpu
from jax.sharding import PartitionSpec as P

EPS = 1e-06
NEG = -1e30
LOG2E = math.log2(math.e)
F32 = jnp.float32
BF16 = jnp.bfloat16
MESH = pl.DeviceIdType.MESH
NT = (((1,), (1,)), ((), ()))


def nt(a, b):
    return lax.dot_general(a, b, NT, preferred_element_type=F32)


def nn(a, b):
    return jnp.dot(a, b, preferred_element_type=F32)


def eye(n):
    a = lax.broadcasted_iota(jnp.int32, (n, n), 0)
    b = lax.broadcasted_iota(jnp.int32, (n, n), 1)
    return (a == b).astype(F32).astype(BF16)


def kernel(
    zn,
    yn,
    tn,
    res_ref,
    qs_ref,
    ks_ref,
    vs_ref,
    ql_ref,
    kl_ref,
    vl_ref,
    gates_ref,
    wos_ref,
    wol_ref,
    gain_ref,
    wg_ref,
    wu_ref,
    cg_ref,
    cu_ref,
    wd_ref,
    out_ref,
    gat,
    kv,
    qin,
    wa,
    wb,
    cums,
    bias,
    kk,
    acc,
    stat,
    oout,
    oin,
    sout,
    sin,
    fpo,
    fpi,
    dno,
    dni,
    first,
    ext,
    halo_out,
    halo_in,
    ebuf,
    hid,
    gat_s,
    gat_r,
    kv_s,
    kv_r,
    q_s,
    q_r,
    w1_s,
    w1_r,
    w2_s,
    w2_r,
    o_s,
    o_r,
    st_s,
    st_r,
    fp_s,
    fp_r,
    n_s,
    n_r,
    d_s,
    d_r,
    h_s,
    h_r,
):
    sp = lax.axis_index("sp")
    tp = lax.axis_index("tp")
    z = sp // yn
    y = sp - z * yn
    tok = ks_ref.shape[0]
    wrows = wg_ref.shape[0]
    half = wa.shape[3]
    own = res_ref.shape[0]
    d = res_ref.shape[1]
    hy, hz = yn // 2, zn // 2
    sends = []

    def yid(dy):
        return (z * yn + lax.rem(y + dy + yn, yn), tp)

    def zid(dz):
        return (lax.rem(z + dz + zn, zn) * yn + y, tp)

    def tid(dt):
        return (sp, lax.rem(tp + dt, tn))

    def rc(src, dst, ss, rs, dev):
        return pltpu.make_async_remote_copy(
            src_ref=src, dst_ref=dst, send_sem=ss, recv_sem=rs, device_id=dev, device_id_type=MESH
        )

    def send(src, dst, ss, rs, dev):
        c = rc(src, dst, ss, rs, dev)
        c.start()
        sends.append(c)

    def landed(dst, ss, rs):
        rc(dst, dst, ss, rs, yid(1)).wait_recv()

    barrier = pltpu.get_barrier_semaphore()
    for i in range(1, yn):
        pl.semaphore_signal(barrier, inc=1, device_id=yid(i), device_id_type=MESH)
    for i in range(1, zn):
        pl.semaphore_signal(barrier, inc=1, device_id=zid(i), device_id_type=MESH)
    for i in range(1, tn):
        pl.semaphore_signal(barrier, inc=1, device_id=tid(i), device_id_type=MESH)

    @pl.when(sp > 0)
    def _():
        pl.semaphore_signal(barrier, inc=1, device_id=(sp - 1, tn - 1), device_id_type=MESH)

    row = gates_ref[...]
    lane = lax.broadcasted_iota(jnp.int32, row.shape, 1)
    shift = 1
    while shift < tok:
        row = row + jnp.where(lane >= shift, pltpu.roll(row, shift, 1), 0.0)
        shift *= 2
    gat[y] = row
    kv[y, 0] = ks_ref[...]
    kv[y, 1] = kl_ref[...]
    unit = eye(tok)
    kv[y, 2] = nt(unit, vs_ref[...]).astype(BF16)
    kv[y, 3] = nt(unit, vl_ref[...]).astype(BF16)
    qin[0, 0] = qs_ref[...]
    qin[0, 1] = ql_ref[...]
    wdt = nt(eye(wrows), wd_ref[...]).astype(BF16)
    for h, w in enumerate((wa, wb)):
        cols = slice(h * half, (h + 1) * half)
        w[z, y, 0:wrows] = wg_ref[:, cols]
        w[z, y, wrows : 2 * wrows] = wu_ref[:, cols]
        w[z, y, 2 * wrows : 3 * wrows] = wdt[:, cols]

    extra = jnp.where(jnp.logical_and(tp == tn - 1, sp < zn * yn - 1), tn, 0)
    pl.semaphore_wait(barrier, yn + zn + tn - 3 + extra)

    for i in range(1, yn):
        send(gat.at[y], gat.at[y], gat_s.at[i], gat_r.at[i], yid(i))

    def kv_send(way, s, part):
        k = way * hy + s - 1
        o = lax.rem(y + (s - 1) * (1 if way else -1) + yn, yn)
        sl = kv.at[o, pl.ds(2 * part, 2)]
        send(sl, sl, kv_s.at[k, part], kv_r.at[k, part], yid(-1 if way else 1))

    def kv_wait(way, s, part):
        k = way * hy + s - 1
        o = lax.rem(y + s * (1 if way else -1) + yn, yn)
        landed(kv.at[o, pl.ds(2 * part, 2)], kv_s.at[k, part], kv_r.at[k, part])

    def w1_ref(axis, o):
        return wa.at[z, o] if axis == 0 else wb.at[o, y]

    def w1_part(ref, s, way, n):
        if s < n // 2:
            return ref
        step = ref.shape[0] // 2
        return ref.at[pl.ds(way * step, step)]

    def w1_send(axis, way, s):
        n, me = (yn, y) if axis == 0 else (zn, z)
        k = way * (n // 2) + s - 1
        o = lax.rem(me + (s - 1) * (1 if way else -1) + n, n)
        sl = w1_part(w1_ref(axis, o), s, way, n)
        to = (yid if axis == 0 else zid)(-1 if way else 1)
        send(sl, sl, w1_s.at[axis, k], w1_r.at[axis, k], to)

    def w1_wait(axis, way, s):
        n, me = (yn, y) if axis == 0 else (zn, z)
        k = way * (n // 2) + s - 1
        o = lax.rem(me + s * (1 if way else -1) + n, n)
        landed(w1_part(w1_ref(axis, o), s, way, n), w1_s.at[axis, k], w1_r.at[axis, k])

    def w2_part(axis, o, s, way, part):
        n, m = (zn, yn) if axis == 0 else (yn, zn)
        rows = pl.ds(0, 2 * wrows) if part == 0 else pl.ds(2 * wrows, wrows)
        if s < n // 2:
            span = pl.ds(0, m)
        else:
            span = pl.ds(way * (m // 2), m // 2)
        return wa.at[o, span, rows] if axis == 0 else wb.at[span, o, rows]

    def w2_send(axis, way, s, part):
        n, me = (zn, z) if axis == 0 else (yn, y)
        k = way * (n // 2) + s - 1
        o = lax.rem(me + (s - 1) * (1 if way else -1) + n, n)
        sl = w2_part(axis, o, s, way, part)
        to = (zid if axis == 0 else yid)(-1 if way else 1)
        send(sl, sl, w2_s.at[axis, k, part], w2_r.at[axis, k, part], to)

    def w2_wait(axis, way, s, part):
        n, me = (zn, z) if axis == 0 else (yn, y)
        k = way * (n // 2) + s - 1
        o = lax.rem(me + s * (1 if way else -1) + n, n)
        sl = w2_part(axis, o, s, way, part)
        landed(sl, w2_s.at[axis, k, part], w2_r.at[axis, k, part])

    def w2_step(axis, s, part):
        n = zn if axis == 0 else yn
        for way in (0, 1):
            if s > 1:
                w2_wait(axis, way, s - 1, part)
            if s <= n // 2:
                w2_send(axis, way, s, part)

    for part in (0, 1):
        for way in (0, 1):
            if hy > 1 or part == way:
                kv_send(way, 1, part)
    for i in range(1, zn):

        @pl.when(z - i >= 0)
        def _():
            rc(qin.at[0], qin.at[i], q_s.at[i], q_r.at[i], (sp - i * yn, tp)).start()

    for way in (0, 1):
        w1_send(1, way, 1)
        w1_send(0, way, 1)

    for i in range(1, yn):
        landed(gat.at[lax.rem(y - i + yn, yn)], gat_s.at[i], gat_r.at[i])
    before = jnp.zeros((8, tok), F32)
    for i in range(yn):
        block = gat[i]
        cums[i] = (before + block) * LOG2E
        before = before + jnp.broadcast_to(block[:, tok - 1 : tok], block.shape)
    total = before * LOG2E
    for i in range(1, zn):

        @pl.when(z + i < zn)
        def _():
            landed(qin.at[i], q_s.at[i], q_r.at[i])

    scales = (64 ** (-0.5) * LOG2E, 64 ** (-0.5) * LOG2E, 128 ** (-0.5) * LOG2E)
    spans = ((0, 64), (64, 128), (128, 256))

    def attend(o, mode):
        key_lane = lax.broadcasted_iota(jnp.int32, (tok, 128), 1)
        ksm = kv[o, 0]
        zero = jnp.zeros_like(ksm)
        kk[0:tok] = jnp.where(key_lane < 64, ksm, zero)
        kk[tok : 2 * tok] = jnp.where(key_lane < 64, zero, ksm)
        cum = cums[o]
        for h in range(3):
            bias[h] = -jnp.broadcast_to(cum[h : h + 1, :], (tok, tok)).T

        def one(i, masked):
            qsm = qin[i, 0]
            qla = qin[i, 1]
            raw = nt(kk[...], qsm)
            rawl = nt(kv[o, 1], qla)
            for h in range(3):
                s = raw[h * tok : (h + 1) * tok] if h < 2 else rawl
                s = s * scales[h] + bias[h]
                if masked:
                    a = lax.broadcasted_iota(jnp.int32, s.shape, 0)
                    b = lax.broadcasted_iota(jnp.int32, s.shape, 1)
                    s = jnp.where(a <= b, s, NEG)
                top = jnp.max(s, axis=0, keepdims=True)
                if mode > 0:
                    old = stat[i, h : h + 1]
                    top = jnp.maximum(old, top)
                    fade = jnp.exp2(old - top)
                p = jnp.exp2(s - top)
                den = jnp.sum(p, axis=0, keepdims=True)
                lo, hi = spans[h]
                vt = kv[o, 2, lo:hi] if h < 2 else kv[o, 3]
                part = nn(vt, p.astype(BF16))
                if mode > 0:
                    den = den + fade * stat[i, 3 + h : 4 + h]
                    part = part + fade * acc[i, lo:hi]
                stat[i, h : h + 1] = top
                stat[i, 3 + h : 4 + h] = den
                acc[i, lo:hi] = part

        def step(i, c):
            one(i, False)
            if mode == 2:

                @pl.when(i > 0)
                def _():
                    oout[i] = acc[i].astype(BF16)
                    sout[i, 0:8] = stat[i]
                    sout[i, 8:16] = total
                    to = (sp + i * yn, tp)
                    rc(oout.at[i], oin.at[i], o_s.at[i], o_r.at[i], to).start()
                    rc(sout.at[i], sin.at[i], st_s.at[i], st_r.at[i], to).start()

            return c

        if mode == 0:
            one(0, True)
            lax.fori_loop(1, zn - z, step, 0)
        else:
            lax.fori_loop(jnp.where(o < y, 0, 1), zn - z, step, 0)

    attend(y, 0)
    for s in range(1, hy + 1):
        for part in (0, 1):
            for way in (0, 1):
                if s < hy or part == way:
                    kv_wait(way, s, part)
                if s + 1 < hy or (s + 1 == hy and part == way):
                    kv_send(way, s + 1, part)
        for axis, n in ((1, zn), (0, yn)):
            for way in (0, 1):
                if s <= n // 2:
                    w1_wait(axis, way, s)
                if s + 1 <= n // 2:
                    w1_send(axis, way, s + 1)
        if s == hy:
            for axis in (0, 1):
                for part in (0, 1):
                    w2_step(axis, 1, part)
            attend(lax.rem(y + hy, yn), 2)
        else:
            attend(lax.rem(y - s + yn, yn), 1)
            attend(lax.rem(y + s, yn), 1)

    def merge(i, gap):
        landed(oin.at[i], o_s.at[i], o_r.at[i])
        landed(sin.at[i], st_s.at[i], st_r.at[i])
        gap = gap + sin[i, 8:16]
        for h in range(3):
            lo, hi = spans[h]
            old = stat[0, h : h + 1]
            new = sin[i, h : h + 1] + gap[h : h + 1]
            top = jnp.maximum(old, new)
            a = jnp.exp2(old - top)
            b = jnp.exp2(new - top)
            stat[0, h : h + 1] = top
            stat[0, 3 + h : 4 + h] = a * stat[0, 3 + h : 4 + h] + b * sin[i, 3 + h : 4 + h]
            acc[0, lo:hi] = a * acc[0, lo:hi] + b * oin[i, lo:hi].astype(F32)
        return gap

    lax.fori_loop(1, z + 1, merge, jnp.zeros((8, tok), F32))
    normed = []
    for h in range(3):
        lo, hi = spans[h]
        att = acc[0, lo:hi] / stat[0, 3 + h : 4 + h]
        mean = jnp.mean(att * att, axis=0, keepdims=True)
        normed.append(att * lax.rsqrt(mean + EPS))
    nsm = jnp.concatenate(normed[:2], axis=0).T.astype(BF16)
    nla = normed[2].T.astype(BF16)
    width = min(512, d)
    for c in range(d // width):
        cols = slice(c * width, (c + 1) * width)
        fpo[:, cols] = (nn(nsm, wos_ref[:, cols]) + nn(nla, wol_ref[:, cols])).astype(BF16)

    def mine(ref, t):
        return ref.at[pl.ds(pl.multiple_of(t * own, own), own)]

    for i in range(1, tn):
        send(mine(fpo, lax.rem(tp + i, tn)), fpi.at[i], fp_s.at[i], fp_r.at[i], tid(i))
    for axis in (0, 1):
        for part in (0, 1):
            w2_step(axis, 2, part)
    value = res_ref[...].astype(F32) + mine(fpo, tp)[...].astype(F32)
    for i in range(1, tn):
        landed(fpi.at[i], fp_s.at[i], fp_r.at[i])
        value = value + fpi[i].astype(F32)
    first[...] = value
    mean = jnp.mean(value * value, axis=1, keepdims=True)
    normal = value * lax.rsqrt(mean + EPS) * gain_ref[...]
    ext[0:16] = jnp.zeros((16, d), BF16)
    place = ext.at[pl.ds(pl.multiple_of(16 + tp * own, 16), own)]
    place[...] = normal.astype(BF16)
    for i in range(1, tn):
        send(place, place, n_s.at[i], n_r.at[i], tid(i))
    hw = d // 8

    @pl.when(jnp.logical_and(tp == tn - 1, sp < zn * yn - 1))
    def _():
        rows = [normal[own - 2 : own, c * hw : (c + 1) * hw] for c in range(8)]
        halo_out[...] = jnp.concatenate(rows, axis=0).astype(BF16)
        for i in range(tn):
            rc(halo_out, halo_in, h_s.at[i], h_r, (sp + 1, i)).start()

    for axis in (0, 1):
        for part in (0, 1):
            w2_step(axis, 3, part)

    @pl.when(sp > 0)
    def _():
        landed(halo_in, h_s.at[0], h_r)
        block = halo_in[...].astype(F32)
        for c in range(8):
            pad = jnp.zeros((14, hw), F32)
            rim = jnp.concatenate([pad, block[2 * c : 2 * c + 2]], axis=0)
            ext[0:16, c * hw : (c + 1) * hw] = rim.astype(BF16)

    for i in range(1, tn):
        src = lax.rem(tp - i + tn, tn)
        landed(ext.at[pl.ds(pl.multiple_of(16 + src * own, 16), own)], n_s.at[i], n_r.at[i])
    for axis in (0, 1):
        for part in (0, 1):
            w2_step(axis, 4, part)
    for s in (hz + 1,):
        w2_step(0, s, 0)
    for s in (hy + 1,):
        w2_step(1, s, 0)

    count = zn * yn
    for h, (w, _n) in enumerate(((wa, 0), (wb, 1))):
        cols = slice(h * half, (h + 1) * half)
        conv = []
        for j, taps in ((0, cg_ref), (1, cu_ref)):
            weight = w[:, :, j * wrows : (j + 1) * wrows].reshape(count * wrows, half)
            ebuf[j] = nn(ext[...], weight).astype(BF16).astype(F32)
            conv.append(
                taps[0:1, cols] * ebuf[j, 14 : 14 + tok]
                + taps[1:2, cols] * ebuf[j, 15 : 15 + tok]
                + taps[2:3, cols] * ebuf[j, 16 : 16 + tok]
            )
        hid[h] = (conv[0] / (1.0 + jnp.exp(-conv[0])) * conv[1]).astype(BF16)

    w2_step(0, hz + 1, 1)
    w2_step(1, hy + 1, 1)
    zs = max(1, zn // 4)
    for c in range(zn // zs):
        span = zs * yn * wrows
        total_down = None
        for h, w in enumerate((wa, wb)):
            weight = w[c * zs : (c + 1) * zs, :, 2 * wrows : 3 * wrows].reshape(span, half)
            term = nt(hid[h], weight)
            total_down = term if total_down is None else total_down + term
        dno[:, c * span : (c + 1) * span] = total_down.astype(BF16)
    for i in range(1, tn):
        send(mine(dno, lax.rem(tp + i, tn)), dni.at[i], d_s.at[i], d_r.at[i], tid(i))
    value = first[...] + mine(dno, tp)[...].astype(F32)
    for i in range(1, tn):
        landed(dni.at[i], d_s.at[i], d_r.at[i])
        value = value + dni[i].astype(F32)
    out_ref[...] = value.astype(BF16)

    for c in sends:
        c.wait_send()
    for i in range(1, zn):

        @pl.when(z - i >= 0)
        def _():
            rc(qin.at[0], qin.at[i], q_s.at[i], q_r.at[i], yid(1)).wait_send()

        @pl.when(z + i < zn)
        def _():
            rc(oout.at[i], oin.at[i], o_s.at[i], o_r.at[i], yid(1)).wait_send()
            rc(sout.at[i], sin.at[i], st_s.at[i], st_r.at[i], yid(1)).wait_send()

    @pl.when(jnp.logical_and(tp == tn - 1, sp < zn * yn - 1))
    def _():
        for i in range(tn):
            rc(halo_out, halo_in, h_s.at[i], h_r, yid(1)).wait_send()


def body(
    sizes,
    residual,
    q_small,
    k_small,
    v_small,
    q_large,
    k_large,
    v_large,
    forget_small,
    forget_large,
    w_out_small,
    w_out_large,
    norm_gain,
    w_gate,
    w_up,
    conv_gate,
    conv_up,
    w_down,
):
    zn, yn, tn = sizes
    tok = q_small.shape[0]
    own, d = residual.shape
    wrows, ff = w_gate.shape
    half = ff // 2
    gates = jnp.concatenate([forget_small, forget_large], axis=1)
    gates = jnp.pad(jax.nn.log_sigmoid(gates).T, ((0, 5), (0, 0)))
    dma = pltpu.SemaphoreType.DMA
    hy, hz = yn // 2, zn // 2
    scratch = [
        pltpu.VMEM((yn, 8, tok), F32),
        pltpu.VMEM((yn, 4, tok, 128), BF16),
        pltpu.VMEM((zn, 2, tok, 128), BF16),
        pltpu.VMEM((zn, yn, 3 * wrows, half), BF16),
        pltpu.VMEM((zn, yn, 3 * wrows, half), BF16),
        pltpu.VMEM((yn, 8, tok), F32),
        pltpu.VMEM((3, tok, tok), F32),
        pltpu.VMEM((2 * tok, 128), BF16),
        pltpu.VMEM((zn, 256, tok), F32),
        pltpu.VMEM((zn, 8, tok), F32),
        pltpu.VMEM((zn, 256, tok), BF16),
        pltpu.VMEM((zn, 256, tok), BF16),
        pltpu.VMEM((zn, 16, tok), F32),
        pltpu.VMEM((zn, 16, tok), F32),
        pltpu.VMEM((tok, d), BF16),
        pltpu.VMEM((tn, own, d), BF16),
        pltpu.VMEM((tok, d), BF16),
        pltpu.VMEM((tn, own, d), BF16),
        pltpu.VMEM((own, d), F32),
        pltpu.VMEM((tok + 16, d), BF16),
        pltpu.VMEM((16, d // 8), BF16),
        pltpu.VMEM((16, d // 8), BF16),
        pltpu.VMEM((2, tok + 16, half), F32),
        pltpu.VMEM((2, tok, half), BF16),
        dma((yn,)),
        dma((yn,)),
        dma((yn, 2)),
        dma((yn, 2)),
        dma((zn,)),
        dma((zn,)),
        dma((2, max(yn, zn))),
        dma((2, max(yn, zn))),
        dma((2, max(yn, zn), 2)),
        dma((2, max(yn, zn), 2)),
        dma((zn,)),
        dma((zn,)),
        dma((zn,)),
        dma((zn,)),
        dma((tn,)),
        dma((tn,)),
        dma((tn,)),
        dma((tn,)),
        dma((tn,)),
        dma((tn,)),
        dma((tn,)),
        dma,
    ]
    return pl.pallas_call(
        functools.partial(kernel, zn, yn, tn),
        out_shape=jax.ShapeDtypeStruct((own, d), BF16),
        in_specs=[pl.BlockSpec(memory_space=pltpu.VMEM)] * 16,
        out_specs=pl.BlockSpec(memory_space=pltpu.VMEM),
        scratch_shapes=scratch,
        compiler_params=pltpu.CompilerParams(
            collective_id=0, has_side_effects=True, vmem_limit_bytes=60 * 1024 * 1024
        ),
    )(
        residual,
        q_small,
        k_small,
        v_small,
        q_large,
        k_large,
        v_large,
        gates,
        w_out_small,
        w_out_large,
        norm_gain.reshape(1, d),
        w_gate,
        w_up,
        conv_gate,
        conv_up,
        w_down,
    )


def solution(mesh):
    sp = mesh.shape["sp"]
    yn = math.isqrt(sp)
    zn = sp // yn
    placed = (
        P(("sp", "tp"), None),
        P("sp", "tp"),
        P("sp", "tp"),
        P("sp", "tp"),
        P("sp", "tp"),
        P("sp", "tp"),
        P("sp", "tp"),
        P("sp", "tp"),
        P("sp", "tp"),
        P("tp", None),
        P("tp", None),
        P(),
        P("sp", "tp"),
        P("sp", "tp"),
        P(None, "tp"),
        P(None, "tp"),
        P("tp", "sp"),
    )
    return jax.shard_map(
        functools.partial(body, (zn, yn, mesh.shape["tp"])),
        mesh=mesh,
        in_specs=placed,
        out_specs=P(("sp", "tp"), None),
        check_vma=False,
    )
```

time: 241 us -> 114 us (0.47)
  Pallas kernels: 0 us -> 110 us
  waiting for transfers between devices: 93.3 us -> 0 us
  blocking collectives: 78.5 us -> 0 us
  matrix products: 19.4 us -> 0 us
  between operations: 13.7 us -> 0.01 us
  other arithmetic: 12.5 us -> 0.02 us
  local copies, waits for them, and re-layouts: 15.3 us -> 4.27 us
  starting transfers between devices: 6.38 us -> 0 us
    pallas_call x0 -> x1, Pallas kernels: none -> 110 us  [body(): pl.pallas_call(functools.partial(kernel, zn, yn, tn), out_shape=jax.Shape...]
    all_gather x2 -> x0, waiting for transfers between devices: 92.5 us -> none  [the longest x1 48.6 us: in_one_piece(): whole = lax.all_gather(both, axis, axis=dim, tiled=True)]
    all_gather x1 -> x0, blocking collectives: 47.5 us -> none  [in_one_piece(): whole = lax.all_gather(both, axis, axis=dim, tiled=True)]
    all_to_all x2 -> x0, blocking collectives: 31 us -> none  [sent_and_summed(): parts = lax.all_to_all(in_blocks(array, dim, size), axis, 0, 0, tiled=True)]
    dot_general x9 -> x0, matrix products: 19.4 us -> none  [the longest x2 7.16 us: attend(): jnp.einsum('qhd,khd->qhk', queries, keys, preferred_element_type=jnp.floa...]
    split x6 -> x0, local copies, waits for them, and re-layouts: 13.6 us -> none  [in_one_piece(): jnp.split(whole, [sum(widths[:k]) for k in range(1, len(widths))], axis=a...]
    all_to_all x1 -> x0, starting transfers between devices: 4.43 us -> none  [sent_to_all(): lax.all_to_all(jnp.broadcast_to(array[None], (size, *array.shape)), axis,...]
    unnamed x25 -> x6, local copies, waits for them, and re-layouts: 0.25 us -> 3.66 us
  transfers between devices with their start and end apart: 4 -> 0, of which waited for: 3 -> 0; matrix products, arithmetic and copies ran while one was open for 16% -> 0% of each run, Pallas kernels for 0% -> 0%
where the time goes in v1:
time: 114 us
  Pallas kernels  110 us (96%)
  local copies, waits for them, and re-layouts  4.27 us (4%)
    pallas_call x1, Pallas kernels, body(): pl.pallas_call(functools.partial(kernel, zn, yn, tn), out_shape=jax.Shape...  110 us
    unnamed x6, local copies, waits for them, and re-layouts  3.66 us

profile of v1, /device:TPU:1, one launch (start us, length us, event | category | flops | bytes accessed | tf_op | source)
XLA Modules:
  0.0 114.0 jit_solution(18420609075379537252)
XLA Ops:
  0.0 0.0 copy-start.1
  0.0 0.0 copy-start
  0.0 0.7 copy-done.1
  0.7 0.0 copy-done
  0.7 0.6 pad.4.gates_ref
  1.3 1.5 %copy.18.wd_ref = bf16[512,32]{1,0:T(8,128)(2,1)} copy(bf16[512,32]{0,1:T(8,128)(2,1)} %param.33) | data formatting | bytes 65536 | tf_op args[16]
  2.8 109.7 %shard_map.163 = bf16[16,2048]{1,0:T(8,128)(2,1)} custom-call(bf16[16,2048]{1,0:T(8,128)(2,1)} %res_ref.1, bf16[128,128]{1,0:T(8,128)(2,1)} %qs_ref.1, bf16[128,128]{1,0:T(8,128)(2,1)} %ks_ref.1, bf16[128,128]{1,0:T(8,128)(2,1)} %vs_ref.1, bf16[128,128]{1,0:T(8,128)(2,1)} %ql_ref.1, bf16[128,128]{1,0:T(8,128)(2,1)} %kl_ref.1, bf16[128,128]{1,0:T(8,128)(2,1)} %vl_ref.1, ...), custom_call_target="tpu_custom_call" | custom-call | tf_op jit(solution)/shard_map/pallas_call | solution.py:567
  112.6 1.5 %copy.20 = bf16[16,2048]{1,0:T(8,128)(2,1)} copy(bf16[16,2048]{1,0:T(8,128)(2,1)} %shard_map.163) | data formatting | bytes 131072
  (1 shorter events, 0.0 us)
Async XLA Ops:
  0.0 0.7 copy-start.1
  0.0 0.7 copy-start

commit v2 on v1

v2 whole, which is shorter than its diff:
```python
import functools
import math

import jax
import jax.numpy as jnp
from jax import lax
from jax.experimental import pallas as pl
from jax.experimental.pallas import tpu as pltpu
from jax.sharding import PartitionSpec as P

EPS = 1e-06
NEG = -1e30
LOG2E = math.log2(math.e)
F32 = jnp.float32
BF16 = jnp.bfloat16
MESH = pl.DeviceIdType.MESH
NT = (((1,), (1,)), ((), ()))


def nt(a, b):
    return lax.dot_general(a, b, NT, preferred_element_type=F32)


def nn(a, b):
    return jnp.dot(a, b, preferred_element_type=F32)


def eye(n):
    a = lax.broadcasted_iota(jnp.int32, (n, n), 0)
    b = lax.broadcasted_iota(jnp.int32, (n, n), 1)
    return (a == b).astype(F32).astype(BF16)


def kernel(
    zn,
    yn,
    tn,
    res_ref,
    qs_ref,
    ks_ref,
    vs_ref,
    ql_ref,
    kl_ref,
    vl_ref,
    fs_ref,
    fl_ref,
    wos_hbm,
    wol_hbm,
    gain_ref,
    wg_ref,
    wu_ref,
    cg_ref,
    cu_ref,
    wd_ref,
    out_ref,
    wos_ref,
    wol_ref,
    gat,
    gatz,
    ty,
    tz,
    wa,
    wb,
    cums,
    biass,
    biasl,
    edge,
    kks,
    kkl,
    vvs,
    vvl,
    accs,
    accl,
    stats,
    statl,
    oout,
    oin,
    sout,
    sin,
    fpo,
    fpi,
    dno,
    dni,
    first,
    ext,
    halo_out,
    halo_in,
    ebuf,
    hid,
    loc_s,
    gat_s,
    gat_r,
    t_s,
    t_r,
    w1_s,
    w1_r,
    w2_s,
    w2_r,
    o_s,
    o_r,
    st_s,
    st_r,
    fp_s,
    fp_r,
    n_s,
    n_r,
    d_s,
    d_r,
    h_s,
    h_r,
):
    sp = lax.axis_index("sp")
    tp = lax.axis_index("tp")
    z = sp // yn
    y = sp - z * yn
    tok = ks_ref.shape[0]
    wrows = wg_ref.shape[0]
    half = wa.shape[3]
    own = res_ref.shape[0]
    d = res_ref.shape[1]
    hy, hz = yn // 2, zn // 2
    sends = []

    def yid(dy):
        return (z * yn + lax.rem(y + dy + yn, yn), tp)

    def zid(dz):
        return (lax.rem(z + dz + zn, zn) * yn + y, tp)

    def tid(dt):
        return (sp, lax.rem(tp + dt, tn))

    def rc(src, dst, ss, rs, dev):
        return pltpu.make_async_remote_copy(
            src_ref=src, dst_ref=dst, send_sem=ss, recv_sem=rs, device_id=dev, device_id_type=MESH
        )

    def send(src, dst, ss, rs, dev):
        c = rc(src, dst, ss, rs, dev)
        c.start()
        sends.append(c)

    def landed(dst, ss, rs):
        rc(dst, dst, ss, rs, yid(1)).wait_recv()

    barrier = pltpu.get_barrier_semaphore()
    for i in range(1, yn):
        pl.semaphore_signal(barrier, inc=1, device_id=yid(i), device_id_type=MESH)
    for i in range(1, zn):
        pl.semaphore_signal(barrier, inc=1, device_id=zid(i), device_id_type=MESH)
    for i in range(1, tn):
        pl.semaphore_signal(barrier, inc=1, device_id=tid(i), device_id_type=MESH)

    @pl.when(sp > 0)
    def _():
        pl.semaphore_signal(barrier, inc=1, device_id=(sp - 1, tn - 1), device_id_type=MESH)

    loads = [
        pltpu.make_async_copy(wos_hbm, wos_ref, loc_s.at[0]),
        pltpu.make_async_copy(wol_hbm, wol_ref, loc_s.at[1]),
    ]
    for c in loads:
        c.start()

    def log_gate(x):
        u = jnp.exp(-jnp.abs(x))
        series = u * (1.0 - u * (0.5 - u * (1.0 / 3.0 - u * 0.25)))
        return jnp.minimum(x, 0.0) - jnp.where(u < 0.01, series, jnp.log(1.0 + u))

    row = jnp.concatenate(
        [log_gate(fs_ref[...]), log_gate(fl_ref[...]), jnp.zeros((5, tok), F32)], axis=0
    )
    lane = lax.broadcasted_iota(jnp.int32, row.shape, 1)
    shift = 1
    while shift < tok:
        row = row + jnp.where(lane >= shift, pltpu.roll(row, shift, 1), 0.0)
        shift *= 2
    gat[y] = row
    unit = eye(tok)
    ty[y, 0] = ks_ref[...]
    ty[y, 1] = nt(unit, vs_ref[...]).astype(BF16)
    ty[y, 2] = ql_ref[...]
    tz[z, 0] = kl_ref[...]
    tz[z, 1] = nt(unit, vl_ref[...]).astype(BF16)
    tz[z, 2] = qs_ref[...]
    for h, w in enumerate((wa, wb)):
        cols = slice(h * half, (h + 1) * half)
        w[z, y, 0:wrows] = wg_ref[:, cols]
        w[z, y, wrows : 2 * wrows] = wu_ref[:, cols]
        w[z, y, 2 * wrows : 3 * wrows] = wd_ref[:, cols]
    ext[0:16] = jnp.zeros((16, d), BF16)

    extra = jnp.where(jnp.logical_and(tp == tn - 1, sp < zn * yn - 1), tn, 0)
    pl.semaphore_wait(barrier, yn + zn + tn - 3 + extra)

    for i in range(1, yn):
        send(gat.at[y], gat.at[y], gat_s.at[0, i], gat_r.at[0, i], yid(i))

    def part_of(ref, s, way, n, dim):
        if s < n // 2:
            return ref
        step = ref.shape[dim] // 2
        cut = pl.ds(way * step, step)
        return ref.at[cut] if dim == 0 else ref.at[:, cut]

    def ring(axis, way, s, kind, start):
        n, me = (yn, y) if axis == 0 else (zn, z)
        k = way * (n // 2) + s - 1
        hop = s - 1 if start else s
        o = lax.rem(me + hop * (1 if way else -1) + n, n)
        if kind == 0:
            ref = part_of((ty if axis == 0 else tz).at[o], s, way, n, 1)
            ss, rs = t_s.at[axis, k], t_r.at[axis, k]
        else:
            ref = part_of(wa.at[z, o] if axis == 0 else wb.at[o, y], s, way, n, 0)
            ss, rs = w1_s.at[axis, k], w1_r.at[axis, k]
        if start:
            send(ref, ref, ss, rs, (yid if axis == 0 else zid)(-1 if way else 1))
        else:
            landed(ref, ss, rs)

    def w2_part(axis, o, s, way, part):
        n, m = (zn, yn) if axis == 0 else (yn, zn)
        rows = pl.ds(0, 2 * wrows) if part == 0 else pl.ds(2 * wrows, wrows)
        if s < n // 2:
            span = pl.ds(0, m)
        else:
            span = pl.ds(way * (m // 2), m // 2)
        return wa.at[o, span, rows] if axis == 0 else wb.at[span, o, rows]

    def w2_send(axis, way, s, part):
        n, me = (zn, z) if axis == 0 else (yn, y)
        k = way * (n // 2) + s - 1
        o = lax.rem(me + (s - 1) * (1 if way else -1) + n, n)
        sl = w2_part(axis, o, s, way, part)
        to = (zid if axis == 0 else yid)(-1 if way else 1)
        send(sl, sl, w2_s.at[axis, k, part], w2_r.at[axis, k, part], to)

    def w2_wait(axis, way, s, part):
        n, me = (zn, z) if axis == 0 else (yn, y)
        k = way * (n // 2) + s - 1
        o = lax.rem(me + s * (1 if way else -1) + n, n)
        sl = w2_part(axis, o, s, way, part)
        landed(sl, w2_s.at[axis, k, part], w2_r.at[axis, k, part])

    def w2_step(s, part):
        for axis, n in ((0, zn), (1, yn)):
            for way in (0, 1):
                if 1 < s <= n // 2 + 1:
                    w2_wait(axis, way, s - 1, part)
                if s <= n // 2:
                    w2_send(axis, way, s, part)

    for kind in (0, 1):
        for axis in (0, 1):
            for way in (0, 1):
                ring(axis, way, 1, kind, True)

    for i in range(1, yn):
        landed(gat.at[lax.rem(y - i + yn, yn)], gat_s.at[0, i], gat_r.at[0, i])
    before = jnp.zeros((8, tok), F32)
    for i in range(yn):
        block = gat[i]
        cums[i] = (before + block) * LOG2E
        before = before + jnp.broadcast_to(block[:, tok - 1 : tok], block.shape)
    gatz[z, 0:8] = cums[y]
    gatz[z, 8:16] = before * LOG2E
    for i in range(1, zn):
        send(gatz.at[z], gatz.at[z], gat_s.at[1, i], gat_r.at[1, i], zid(i))
    for i in range(yn):
        for h in range(2):
            column = -jnp.broadcast_to(cums[i, h : h + 1, :], (tok, tok)).T
            biass[h, i * tok : (i + 1) * tok] = column

    for s in range(1, max(hy, hz) + 1):
        for kind in (0, 1):
            for axis, n in ((0, yn), (1, zn)):
                for way in (0, 1):
                    if s <= n // 2:
                        ring(axis, way, s, kind, False)
                    if s + 1 <= n // 2:
                        ring(axis, way, s + 1, kind, True)
        if s == 1:
            for i in range(1, zn):
                landed(gatz.at[lax.rem(z - i + zn, zn)], gat_s.at[1, i], gat_r.at[1, i])
            gap = jnp.zeros((8, tok), F32)
            for i in reversed(range(zn)):
                gap = jnp.where(i < z, gap + gatz[i, 8:16], 0.0)
                away = jnp.where(i > z, -NEG, gatz[i, 2:3] - gap[2:3])
                column = -jnp.broadcast_to(away, (tok, tok)).T
                biasl[i * tok : (i + 1) * tok] = column
            edge[...] = -jnp.broadcast_to(gatz[z, 2:3], (tok, tok)).T

    w2_step(1, 0)
    key_lane = lax.broadcasted_iota(jnp.int32, (tok, 128), 1)
    for i in range(yn):
        rows = slice(i * tok, (i + 1) * tok)
        ksm = ty[i, 0]
        zero = jnp.zeros_like(ksm)
        kks[0, rows] = jnp.where(key_lane < 64, ksm, zero)
        kks[1, rows] = jnp.where(key_lane < 64, zero, ksm)
        vvs[:, rows] = ty[i, 1]
    for i in range(zn):
        rows = slice(i * tok, (i + 1) * tok)
        kkl[rows] = tz[i, 0]
        vvl[:, rows] = tz[i, 1]

    def soft(keys, query, shift, scale, values, keep):
        s = nt(keys, query) * scale + shift
        if keep is not None:
            s = jnp.where(keep, s, NEG)
        top = jnp.max(s, axis=0, keepdims=True)
        p = jnp.exp2(s - top)
        den = jnp.sum(p, axis=0, keepdims=True)
        return top, den, nn(values, p.astype(BF16))

    def small(i, keep):
        query = tz[z + i, 2]
        for h in range(2):
            lo, hi = 64 * h, 64 * h + 64
            top, den, part = soft(
                kks[h], query, biass[h], 64 ** (-0.5) * LOG2E, vvs[lo:hi], keep
            )
            stats[i, h : h + 1] = top
            stats[i, 2 + h : 3 + h] = den
            accs[i, lo:hi] = part

    def small_step(i, c):
        small(i, None)
        oout[0, i] = accs[i].astype(BF16)
        sout[0, i] = stats[i]
        to = (sp + i * yn, tp)
        rc(oout.at[0, i], oin.at[0, i], o_s.at[0, i], o_r.at[0, i], to).start()
        rc(sout.at[0, i], sin.at[0, i], st_s.at[0, i], st_r.at[0, i], to).start()
        return c

    lax.fori_loop(1, zn - z, small_step, 0)

    def large(i, c):
        o = lax.rem(y + i, yn)
        a = lax.broadcasted_iota(jnp.int32, (tok, tok), 0)
        b = lax.broadcasted_iota(jnp.int32, (tok, tok), 1)
        rows = pl.ds(pl.multiple_of(z * tok, tok), tok)
        biasl[rows] = jnp.where(y * tok + a <= o * tok + b, edge[...], NEG)
        top, den, part = soft(
            kkl[...], ty[o, 2], biasl[...], 128 ** (-0.5) * LOG2E, vvl[...], None
        )
        statl[i, 0:1] = top
        statl[i, 2:3] = den
        accl[i] = part

        @pl.when(jnp.logical_and(i > 0, jnp.logical_or(z > 0, o > y)))
        def _():
            oout[1, i] = part.astype(BF16)
            sout[1, i] = statl[i]
            to = (z * yn + o, tp)
            rc(oout.at[1, i], oin.at[1, i], o_s.at[1, i], o_r.at[1, i], to).start()
            rc(sout.at[1, i], sin.at[1, i], st_s.at[1, i], st_r.at[1, i], to).start()

        return c

    lax.fori_loop(0, yn, large, 0)
    a = lax.broadcasted_iota(jnp.int32, (yn * tok, tok), 0)
    b = lax.broadcasted_iota(jnp.int32, (yn * tok, tok), 1)
    small(0, a <= y * tok + b)
    w2_step(1, 1)
    w2_step(2, 0)

    def fold(acc, stat, slot, lo, hi, i, row, gap):
        old = stat[0, row : row + 1]
        new = sin[slot, i, row : row + 1]
        if gap is not None:
            new = new + gap
        top = jnp.maximum(old, new)
        a = jnp.exp2(old - top)
        b = jnp.exp2(new - top)
        stat[0, row : row + 1] = top
        den = a * stat[0, 2 + row : 3 + row] + b * sin[slot, i, 2 + row : 3 + row]
        stat[0, 2 + row : 3 + row] = den
        acc[0, lo:hi] = a * acc[0, lo:hi] + b * oin[slot, i, lo:hi].astype(F32)

    def merge(i, gap):
        landed(oin.at[0, i], o_s.at[0, i], o_r.at[0, i])
        landed(sin.at[0, i], st_s.at[0, i], st_r.at[0, i])
        gap = gap + gatz[z - i, 8:16]
        for h in range(2):
            fold(accs, stats, 0, 64 * h, 64 * h + 64, i, h, gap[h : h + 1])
        return gap

    lax.fori_loop(1, z + 1, merge, jnp.zeros((8, tok), F32))

    def merge_large(i, c):
        @pl.when(jnp.logical_or(z > 0, lax.rem(y - i + yn, yn) < y))
        def _():
            landed(oin.at[1, i], o_s.at[1, i], o_r.at[1, i])
            landed(sin.at[1, i], st_s.at[1, i], st_r.at[1, i])
            fold(accl, statl, 1, 0, 128, i, 0, None)

        return c

    lax.fori_loop(1, yn, merge_large, 0)
    normed = []
    for h in range(3):
        if h < 2:
            att = accs[0, 64 * h : 64 * h + 64] / stats[0, 2 + h : 3 + h]
        else:
            att = accl[0] / statl[0, 2:3]
        mean = jnp.mean(att * att, axis=0, keepdims=True)
        normed.append(att * lax.rsqrt(mean + EPS))
    nsm = jnp.concatenate(normed[:2], axis=0).T.astype(BF16)
    nla = normed[2].T.astype(BF16)
    for c in loads:
        c.wait()
    width = min(512, d)
    for c in range(d // width):
        cols = slice(c * width, (c + 1) * width)
        fpo[:, cols] = (nn(nsm, wos_ref[:, cols]) + nn(nla, wol_ref[:, cols])).astype(BF16)

    def mine(ref, t):
        return ref.at[pl.ds(pl.multiple_of(t * own, own), own)]

    for i in range(1, tn):
        send(mine(fpo, lax.rem(tp + i, tn)), fpi.at[i], fp_s.at[i], fp_r.at[i], tid(i))
    w2_step(2, 1)
    value = res_ref[...].astype(F32) + mine(fpo, tp)[...].astype(F32)
    for i in range(1, tn):
        landed(fpi.at[i], fp_s.at[i], fp_r.at[i])
        value = value + fpi[i].astype(F32)
    first[...] = value
    mean = jnp.mean(value * value, axis=1, keepdims=True)
    normal = value * lax.rsqrt(mean + EPS) * gain_ref[...]
    place = ext.at[pl.ds(pl.multiple_of(16 + tp * own, 16), own)]
    place[...] = normal.astype(BF16)
    for i in range(1, tn):
        send(place, place, n_s.at[i], n_r.at[i], tid(i))
    hw = d // 8

    @pl.when(jnp.logical_and(tp == tn - 1, sp < zn * yn - 1))
    def _():
        rows = [normal[own - 2 : own, c * hw : (c + 1) * hw] for c in range(8)]
        halo_out[...] = jnp.concatenate(rows, axis=0).astype(BF16)
        for i in range(tn):
            rc(halo_out, halo_in, h_s.at[i], h_r, (sp + 1, i)).start()

    w2_step(3, 0)
    w2_step(3, 1)

    @pl.when(sp > 0)
    def _():
        landed(halo_in, h_s.at[0], h_r)
        block = halo_in[...].astype(F32)
        for c in range(8):
            pad = jnp.zeros((14, hw), F32)
            rim = jnp.concatenate([pad, block[2 * c : 2 * c + 2]], axis=0)
            ext[0:16, c * hw : (c + 1) * hw] = rim.astype(BF16)

    for i in range(1, tn):
        src = lax.rem(tp - i + tn, tn)
        landed(ext.at[pl.ds(pl.multiple_of(16 + src * own, 16), own)], n_s.at[i], n_r.at[i])
    w2_step(4, 0)
    w2_step(4, 1)
    w2_step(5, 0)

    count = zn * yn
    for h, (w, _n) in enumerate(((wa, 0), (wb, 1))):
        cols = slice(h * half, (h + 1) * half)
        conv = []
        for j, taps in ((0, cg_ref), (1, cu_ref)):
            weight = w[:, :, j * wrows : (j + 1) * wrows].reshape(count * wrows, half)
            ebuf[j] = nn(ext[...], weight).astype(BF16).astype(F32)
            conv.append(
                taps[0:1, cols] * ebuf[j, 14 : 14 + tok]
                + taps[1:2, cols] * ebuf[j, 15 : 15 + tok]
                + taps[2:3, cols] * ebuf[j, 16 : 16 + tok]
            )
        hid[h] = (conv[0] / (1.0 + jnp.exp(-conv[0])) * conv[1]).astype(BF16)

    w2_step(5, 1)
    zs = max(1, zn // 4)
    for c in range(zn // zs):
        span = zs * yn * wrows
        total_down = None
        for h, w in enumerate((wa, wb)):
            weight = w[c * zs : (c + 1) * zs, :, 2 * wrows : 3 * wrows].reshape(span, half)
            term = nt(hid[h], weight)
            total_down = term if total_down is None else total_down + term
        dno[:, c * span : (c + 1) * span] = total_down.astype(BF16)
    for i in range(1, tn):
        send(mine(dno, lax.rem(tp + i, tn)), dni.at[i], d_s.at[i], d_r.at[i], tid(i))
    value = first[...] + mine(dno, tp)[...].astype(F32)
    for i in range(1, tn):
        landed(dni.at[i], d_s.at[i], d_r.at[i])
        value = value + dni[i].astype(F32)
    out_ref[...] = value.astype(BF16)

    for c in sends:
        c.wait_send()
    for i in range(1, zn):

        @pl.when(z + i < zn)
        def _():
            rc(oout.at[0, i], oin.at[0, i], o_s.at[0, i], o_r.at[0, i], yid(1)).wait_send()
            rc(sout.at[0, i], sin.at[0, i], st_s.at[0, i], st_r.at[0, i], yid(1)).wait_send()

    for i in range(1, yn):

        @pl.when(jnp.logical_or(z > 0, lax.rem(y + i, yn) > y))
        def _():
            rc(oout.at[1, i], oin.at[1, i], o_s.at[1, i], o_r.at[1, i], yid(1)).wait_send()
            rc(sout.at[1, i], sin.at[1, i], st_s.at[1, i], st_r.at[1, i], yid(1)).wait_send()

    @pl.when(jnp.logical_and(tp == tn - 1, sp < zn * yn - 1))
    def _():
        for i in range(tn):
            rc(halo_out, halo_in, h_s.at[i], h_r, yid(1)).wait_send()


def body(
    sizes,
    residual,
    q_small,
    k_small,
    v_small,
    q_large,
    k_large,
    v_large,
    forget_small,
    forget_large,
    w_out_small,
    w_out_large,
    norm_gain,
    w_gate,
    w_up,
    conv_gate,
    conv_up,
    w_down,
):
    zn, yn, tn = sizes
    tok = q_small.shape[0]
    own, d = residual.shape
    wrows, ff = w_gate.shape
    half = ff // 2
    dma = pltpu.SemaphoreType.DMA
    big = max(yn, zn)
    scratch = [
        pltpu.VMEM(w_out_small.shape, BF16),
        pltpu.VMEM(w_out_large.shape, BF16),
        pltpu.VMEM((yn, 8, tok), F32),
        pltpu.VMEM((zn, 16, tok), F32),
        pltpu.VMEM((yn, 3, tok, 128), BF16),
        pltpu.VMEM((zn, 3, tok, 128), BF16),
        pltpu.VMEM((zn, yn, 3 * wrows, half), BF16),
        pltpu.VMEM((zn, yn, 3 * wrows, half), BF16),
        pltpu.VMEM((yn, 8, tok), F32),
        pltpu.VMEM((2, yn * tok, tok), F32),
        pltpu.VMEM((zn * tok, tok), F32),
        pltpu.VMEM((tok, tok), F32),
        pltpu.VMEM((2, yn * tok, 128), BF16),
        pltpu.VMEM((zn * tok, 128), BF16),
        pltpu.VMEM((128, yn * tok), BF16),
        pltpu.VMEM((128, zn * tok), BF16),
        pltpu.VMEM((zn, 128, tok), F32),
        pltpu.VMEM((yn, 128, tok), F32),
        pltpu.VMEM((zn, 8, tok), F32),
        pltpu.VMEM((yn, 8, tok), F32),
        pltpu.VMEM((2, big, 128, tok), BF16),
        pltpu.VMEM((2, big, 128, tok), BF16),
        pltpu.VMEM((2, big, 8, tok), F32),
        pltpu.VMEM((2, big, 8, tok), F32),
        pltpu.VMEM((tok, d), BF16),
        pltpu.VMEM((tn, own, d), BF16),
        pltpu.VMEM((tok, d), BF16),
        pltpu.VMEM((tn, own, d), BF16),
        pltpu.VMEM((own, d), F32),
        pltpu.VMEM((tok + 16, d), BF16),
        pltpu.VMEM((16, d // 8), BF16),
        pltpu.VMEM((16, d // 8), BF16),
        pltpu.VMEM((2, tok + 16, half), F32),
        pltpu.VMEM((2, tok, half), BF16),
        dma((2,)),
        dma((2, big)),
        dma((2, big)),
        dma((2, big)),
        dma((2, big)),
        dma((2, big)),
        dma((2, big)),
        dma((2, big, 2)),
        dma((2, big, 2)),
        dma((2, big)),
        dma((2, big)),
        dma((2, big)),
        dma((2, big)),
        dma((tn,)),
        dma((tn,)),
        dma((tn,)),
        dma((tn,)),
        dma((tn,)),
        dma((tn,)),
        dma((tn,)),
        dma,
    ]
    vmem = pl.BlockSpec(memory_space=pltpu.VMEM)
    hbm = pl.BlockSpec(memory_space=pl.ANY)
    return pl.pallas_call(
        functools.partial(kernel, zn, yn, tn),
        out_shape=jax.ShapeDtypeStruct((own, d), BF16),
        in_specs=[vmem] * 9 + [hbm] * 2 + [vmem] * 6,
        out_specs=pl.BlockSpec(memory_space=pltpu.VMEM),
        scratch_shapes=scratch,
        compiler_params=pltpu.CompilerParams(
            collective_id=0, has_side_effects=True, vmem_limit_bytes=60 * 1024 * 1024
        ),
    )(
        residual,
        q_small,
        k_small,
        v_small,
        q_large,
        k_large,
        v_large,
        forget_small.T,
        forget_large.T,
        w_out_small,
        w_out_large,
        norm_gain.reshape(1, d),
        w_gate,
        w_up,
        conv_gate,
        conv_up,
        w_down.T,
    )


def solution(mesh):
    sp = mesh.shape["sp"]
    yn = math.isqrt(sp)
    zn = sp // yn
    placed = (
        P(("sp", "tp"), None),
        P("sp", "tp"),
        P("sp", "tp"),
        P("sp", "tp"),
        P("sp", "tp"),
        P("sp", "tp"),
        P("sp", "tp"),
        P("sp", "tp"),
        P("sp", "tp"),
        P("tp", None),
        P("tp", None),
        P(),
        P("sp", "tp"),
        P("sp", "tp"),
        P(None, "tp"),
        P(None, "tp"),
        P("tp", "sp"),
    )
    return jax.shard_map(
        functools.partial(body, (zn, yn, mesh.shape["tp"])),
        mesh=mesh,
        in_specs=placed,
        out_specs=P(("sp", "tp"), None),
        check_vma=False,
    )
```

time: 114 us -> 88.9 us (0.78)
  Pallas kernels: 110 us -> 87.2 us
  local copies, waits for them, and re-layouts: 4.27 us -> 1.47 us
    pallas_call x1, Pallas kernels: 110 us -> 87.2 us  [body(): pl.pallas_call(functools.partial(kernel, zn, yn, tn), out_shape=jax.Shape...]
    unnamed x6 -> x1, local copies, waits for them, and re-layouts: 3.66 us -> 1.47 us
where the time goes in v2:
time: 88.9 us; the launch traced here: 88.7 us
  Pallas kernels  87.2 us (98%)
  local copies, waits for them, and re-layouts  1.47 us (2%)
    pallas_call x1, Pallas kernels, body(): pl.pallas_call(functools.partial(kernel, zn, yn, tn), out_shape=jax.Shape...  87.2 us

profile of v2, /device:TPU:1, one launch (start us, length us, event | category | flops | bytes accessed | tf_op | source)
XLA Modules:
  0.0 88.7 jit_solution(12084308131746288409)
XLA Ops:
  0.0 87.2 %shard_map.163 = bf16[16,2048]{1,0:T(8,128)(2,1)} custom-call(bf16[16,2048]{1,0:T(8,128)(2,1)} %res_ref.1, bf16[128,128]{1,0:T(8,128)(2,1)} %qs_ref.1, bf16[128,128]{1,0:T(8,128)(2,1)} %ks_ref.1, bf16[128,128]{1,0:T(8,128)(2,1)} %vs_ref.1, bf16[128,128]{1,0:T(8,128)(2,1)} %ql_ref.1, bf16[128,128]{1,0:T(8,128)(2,1)} %kl_ref.1, bf16[128,128]{1,0:T(8,128)(2,1)} %vl_ref.1, ...), custom_call_target="tpu_custom_call" | custom-call | tf_op jit(solution)/shard_map/pallas_call | solution.py:604
  87.2 1.5 %copy.19 = bf16[16,2048]{1,0:T(8,128)(2,1)} copy(bf16[16,2048]{1,0:T(8,128)(2,1)} %shard_map.163) | data formatting | bytes 131072

commit v3 on v2

--- a/solution.py
+++ b/solution.py
@@ -196,23 +196,22 @@
     for i in range(1, yn):
         send(gat.at[y], gat.at[y], gat_s.at[0, i], gat_r.at[0, i], yid(i))
 
-    def part_of(ref, s, way, n, dim):
-        if s < n // 2:
-            return ref
-        step = ref.shape[dim] // 2
-        cut = pl.ds(way * step, step)
-        return ref.at[cut] if dim == 0 else ref.at[:, cut]
-
     def ring(axis, way, s, kind, start):
         n, me = (yn, y) if axis == 0 else (zn, z)
         k = way * (n // 2) + s - 1
         hop = s - 1 if start else s
         o = lax.rem(me + hop * (1 if way else -1) + n, n)
-        if kind == 0:
-            ref = part_of((ty if axis == 0 else tz).at[o], s, way, n, 1)
-            ss, rs = t_s.at[axis, k], t_r.at[axis, k]
+        last = s == n // 2
+        if kind < 2:
+            if last and kind != way:
+                return
+            ref = (ty if axis == 0 else tz).at[o, :, pl.ds(kind * (tok // 2), tok // 2)]
+            ss, rs = t_s.at[axis, k, kind], t_r.at[axis, k, kind]
         else:
-            ref = part_of(wa.at[z, o] if axis == 0 else wb.at[o, y], s, way, n, 0)
+            ref = wa.at[z, o] if axis == 0 else wb.at[o, y]
+            if last:
+                step = 3 * wrows // 2
+                ref = ref.at[pl.ds(way * step, step)]
             ss, rs = w1_s.at[axis, k], w1_r.at[axis, k]
         if start:
             send(ref, ref, ss, rs, (yid if axis == 0 else zid)(-1 if way else 1))
@@ -251,11 +250,21 @@
                 if s <= n // 2:
                     w2_send(axis, way, s, part)
 
-    for kind in (0, 1):
+    for kind in (0, 1, 2):
         for axis in (0, 1):
             for way in (0, 1):
                 ring(axis, way, 1, kind, True)
 
+    def ring_step(s, kinds):
+        for kind in kinds:
+            for axis, n in ((0, yn), (1, zn)):
+                for way in (0, 1):
+                    if s <= n // 2:
+                        ring(axis, way, s, kind, False)
+                    if s + 1 <= n // 2:
+                        ring(axis, way, s + 1, kind, True)
+
+    ring_step(1, (0, 1))
     for i in range(1, yn):
         landed(gat.at[lax.rem(y - i + yn, yn)], gat_s.at[0, i], gat_r.at[0, i])
     before = jnp.zeros((8, tok), F32)
@@ -267,20 +276,14 @@
     gatz[z, 8:16] = before * LOG2E
     for i in range(1, zn):
         send(gatz.at[z], gatz.at[z], gat_s.at[1, i], gat_r.at[1, i], zid(i))
+    ring_step(1, (2,))
     for i in range(yn):
         for h in range(2):
             column = -jnp.broadcast_to(cums[i, h : h + 1, :], (tok, tok)).T
             biass[h, i * tok : (i + 1) * tok] = column
-
-    for s in range(1, max(hy, hz) + 1):
-        for kind in (0, 1):
-            for axis, n in ((0, yn), (1, zn)):
-                for way in (0, 1):
-                    if s <= n // 2:
-                        ring(axis, way, s, kind, False)
-                    if s + 1 <= n // 2:
-                        ring(axis, way, s + 1, kind, True)
-        if s == 1:
+    for s in range(2, max(hy, hz) + 1):
+        ring_step(s, (0, 1, 2))
+        if s == 2:
             for i in range(1, zn):
                 landed(gatz.at[lax.rem(z - i + zn, zn)], gat_s.at[1, i], gat_r.at[1, i])
             gap = jnp.zeros((8, tok), F32)
@@ -288,10 +291,12 @@
                 gap = jnp.where(i < z, gap + gatz[i, 8:16], 0.0)
                 away = jnp.where(i > z, -NEG, gatz[i, 2:3] - gap[2:3])
                 column = -jnp.broadcast_to(away, (tok, tok)).T
-                biasl[i * tok : (i + 1) * tok] = column
+                for j in range(2):
+                    biasl[j, i * tok : (i + 1) * tok] = column
             edge[...] = -jnp.broadcast_to(gatz[z, 2:3], (tok, tok)).T
 
     w2_step(1, 0)
+    w2_step(1, 1)
     key_lane = lax.broadcasted_iota(jnp.int32, (tok, 128), 1)
     for i in range(yn):
         rows = slice(i * tok, (i + 1) * tok)
@@ -305,66 +310,100 @@
         kkl[rows] = tz[i, 0]
         vvl[:, rows] = tz[i, 1]
 
-    def soft(keys, query, shift, scale, values, keep):
-        s = nt(keys, query) * scale + shift
-        if keep is not None:
-            s = jnp.where(keep, s, NEG)
-        top = jnp.max(s, axis=0, keepdims=True)
-        p = jnp.exp2(s - top)
-        den = jnp.sum(p, axis=0, keepdims=True)
-        return top, den, nn(values, p.astype(BF16))
-
-    def small(i, keep):
-        query = tz[z + i, 2]
+    def soft(keys, queries, shifts, scale, values, limit):
+        raw = nt(keys, queries)
+        tops, dens, ps = [], [], []
+        for j in range(2):
+            s = raw[:, j * tok : (j + 1) * tok] * scale + shifts[j]
+            if limit is not None and j == 0:
+                spot = lax.broadcasted_iota(jnp.int32, s.shape, 0)
+                s = jnp.where(spot <= limit, s, NEG)
+            top = jnp.max(s, axis=0, keepdims=True)
+            p = jnp.exp2(s - top)
+            tops.append(top)
+            dens.append(jnp.sum(p, axis=0, keepdims=True))
+            ps.append(p.astype(BF16))
+        return tops, dens, nn(values, jnp.concatenate(ps, axis=1))
+
+    def two(ref, first_one, n):
+        other = lax.rem(first_one + 1, n)
+        return jnp.concatenate([ref[lax.rem(first_one, n), 2], ref[other, 2]], axis=0)
+
+    def push(slot, i, to):
+        rc(oout.at[slot, i], oin.at[slot, i], o_s.at[slot, i], o_r.at[slot, i], to).start()
+        rc(sout.at[slot, i], sin.at[slot, i], st_s.at[slot, i], st_r.at[slot, i], to).start()
+
+    def small(p, limit):
+        queries = two(tz, z + 2 * p, zn)
         for h in range(2):
             lo, hi = 64 * h, 64 * h + 64
-            top, den, part = soft(
-                kks[h], query, biass[h], 64 ** (-0.5) * LOG2E, vvs[lo:hi], keep
+            shift = biass[h]
+            tops, dens, part = soft(
+                kks[h], queries, (shift, shift), 64 ** (-0.5) * LOG2E, vvs[lo:hi], limit
             )
-            stats[i, h : h + 1] = top
-            stats[i, 2 + h : 3 + h] = den
-            accs[i, lo:hi] = part
-
-    def small_step(i, c):
-        small(i, None)
-        oout[0, i] = accs[i].astype(BF16)
-        sout[0, i] = stats[i]
-        to = (sp + i * yn, tp)
-        rc(oout.at[0, i], oin.at[0, i], o_s.at[0, i], o_r.at[0, i], to).start()
-        rc(sout.at[0, i], sin.at[0, i], st_s.at[0, i], st_r.at[0, i], to).start()
+            for j in range(2):
+                piece = part[:, j * tok : (j + 1) * tok]
+                if limit is not None and j == 0:
+                    stats[0, h : h + 1] = tops[j]
+                    stats[0, 2 + h : 3 + h] = dens[j]
+                    accs[0, lo:hi] = piece
+                else:
+                    sout[0, 2 * p + j, h : h + 1] = tops[j]
+                    sout[0, 2 * p + j, 2 + h : 3 + h] = dens[j]
+                    oout[0, 2 * p + j, lo:hi] = piece.astype(BF16)
+        for j in range(2):
+            if limit is None or j == 1:
+
+                @pl.when(z + 2 * p + j < zn)
+                def _():
+                    push(0, 2 * p + j, (sp + (2 * p + j) * yn, tp))
+
+    def small_step(p, c):
+        small(p, None)
         return c
 
-    lax.fori_loop(1, zn - z, small_step, 0)
-
-    def large(i, c):
-        o = lax.rem(y + i, yn)
+    lax.fori_loop(1, (zn - z + 1) // 2, small_step, 0)
+    small(0, y * tok + lax.broadcasted_iota(jnp.int32, (1, tok), 1))
+
+    def large(p, c):
         a = lax.broadcasted_iota(jnp.int32, (tok, tok), 0)
         b = lax.broadcasted_iota(jnp.int32, (tok, tok), 1)
         rows = pl.ds(pl.multiple_of(z * tok, tok), tok)
-        biasl[rows] = jnp.where(y * tok + a <= o * tok + b, edge[...], NEG)
-        top, den, part = soft(
-            kkl[...], ty[o, 2], biasl[...], 128 ** (-0.5) * LOG2E, vvl[...], None
+        for j in range(2):
+            o = lax.rem(y + 2 * p + j, yn)
+            biasl[j, rows] = jnp.where(y * tok + a <= o * tok + b, edge[...], NEG)
+        tops, dens, part = soft(
+            kkl[...],
+            two(ty, y + 2 * p, yn),
+            (biasl[0], biasl[1]),
+            128 ** (-0.5) * LOG2E,
+            vvl[...],
+            None,
         )
-        statl[i, 0:1] = top
-        statl[i, 2:3] = den
-        accl[i] = part
-
-        @pl.when(jnp.logical_and(i > 0, jnp.logical_or(z > 0, o > y)))
-        def _():
-            oout[1, i] = part.astype(BF16)
-            sout[1, i] = statl[i]
-            to = (z * yn + o, tp)
-            rc(oout.at[1, i], oin.at[1, i], o_s.at[1, i], o_r.at[1, i], to).start()
-            rc(sout.at[1, i], sin.at[1, i], st_s.at[1, i], st_r.at[1, i], to).start()
+        for j in range(2):
+            i = 2 * p + j
+            o = lax.rem(y + i, yn)
+            piece = part[:, j * tok : (j + 1) * tok]
+            sout[1, i, 0:1] = tops[j]
+            sout[1, i, 2:3] = dens[j]
+            oout[1, i] = piece.astype(BF16)
+            if j == 0:
+
+                @pl.when(p == 0)
+                def _():
+                    statl[0, 0:1] = tops[0]
+                    statl[0, 2:3] = dens[0]
+                    accl[0] = piece
+
+            @pl.when(jnp.logical_and(i > 0, jnp.logical_or(z > 0, o > y)))
+            def _():
+                push(1, i, (z * yn + o, tp))
 
         return c
 
-    lax.fori_loop(0, yn, large, 0)
-    a = lax.broadcasted_iota(jnp.int32, (yn * tok, tok), 0)
-    b = lax.broadcasted_iota(jnp.int32, (yn * tok, tok), 1)
-    small(0, a <= y * tok + b)
-    w2_step(1, 1)
+    lax.fori_loop(0, yn // 2, large, 0)
     w2_step(2, 0)
+    w2_step(2, 1)
 
     def fold(acc, stat, slot, lo, hi, i, row, gap):
         old = stat[0, row : row + 1]
@@ -421,7 +460,7 @@
 
     for i in range(1, tn):
         send(mine(fpo, lax.rem(tp + i, tn)), fpi.at[i], fp_s.at[i], fp_r.at[i], tid(i))
-    w2_step(2, 1)
+    w2_step(3, 0)
     value = res_ref[...].astype(F32) + mine(fpo, tp)[...].astype(F32)
     for i in range(1, tn):
         landed(fpi.at[i], fp_s.at[i], fp_r.at[i])
@@ -442,8 +481,8 @@
         for i in range(tn):
             rc(halo_out, halo_in, h_s.at[i], h_r, (sp + 1, i)).start()
 
-    w2_step(3, 0)
     w2_step(3, 1)
+    w2_step(4, 0)
 
     @pl.when(sp > 0)
     def _():
@@ -457,7 +496,6 @@
     for i in range(1, tn):
         src = lax.rem(tp - i + tn, tn)
         landed(ext.at[pl.ds(pl.multiple_of(16 + src * own, 16), own)], n_s.at[i], n_r.at[i])
-    w2_step(4, 0)
     w2_step(4, 1)
     w2_step(5, 0)
 
@@ -553,16 +591,16 @@
         pltpu.VMEM((zn, yn, 3 * wrows, half), BF16),
         pltpu.VMEM((yn, 8, tok), F32),
         pltpu.VMEM((2, yn * tok, tok), F32),
-        pltpu.VMEM((zn * tok, tok), F32),
+        pltpu.VMEM((2, zn * tok, tok), F32),
         pltpu.VMEM((tok, tok), F32),
         pltpu.VMEM((2, yn * tok, 128), BF16),
         pltpu.VMEM((zn * tok, 128), BF16),
         pltpu.VMEM((128, yn * tok), BF16),
         pltpu.VMEM((128, zn * tok), BF16),
-        pltpu.VMEM((zn, 128, tok), F32),
-        pltpu.VMEM((yn, 128, tok), F32),
-        pltpu.VMEM((zn, 8, tok), F32),
-        pltpu.VMEM((yn, 8, tok), F32),
+        pltpu.VMEM((1, 128, tok), F32),
+        pltpu.VMEM((1, 128, tok), F32),
+        pltpu.VMEM((1, 8, tok), F32),
+        pltpu.VMEM((1, 8, tok), F32),
         pltpu.VMEM((2, big, 128, tok), BF16),
         pltpu.VMEM((2, big, 128, tok), BF16),
         pltpu.VMEM((2, big, 8, tok), F32),
@@ -580,8 +618,8 @@
         dma((2,)),
         dma((2, big)),
         dma((2, big)),
-        dma((2, big)),
-        dma((2, big)),
+        dma((2, big, 2)),
+        dma((2, big, 2)),
         dma((2, big)),
         dma((2, big)),
         dma((2, big, 2)),

time: 88.9 us -> 86 us (0.967)
  Pallas kernels: 87.2 us -> 84.3 us
    pallas_call x1, Pallas kernels: 87.2 us -> 84.3 us  [body(): pl.pallas_call(functools.partial(kernel, zn, yn, tn), out_shape=jax.Shape...]
where the time goes in v3:
time: 86 us; the launch traced here: 85.8 us
  Pallas kernels  84.3 us (98%)
  local copies, waits for them, and re-layouts  1.47 us (2%)
    pallas_call x1, Pallas kernels, body(): pl.pallas_call(functools.partial(kernel, zn, yn, tn), out_shape=jax.Shape...  84.3 us

profile of v3, /device:TPU:1, one launch (start us, length us, event | category | flops | bytes accessed | tf_op | source)
XLA Modules:
  0.0 85.8 jit_solution(14434046004418764436)
XLA Ops:
  0.0 84.3 %shard_map.163 = bf16[16,2048]{1,0:T(8,128)(2,1)} custom-call(bf16[16,2048]{1,0:T(8,128)(2,1)} %res_ref.1, bf16[128,128]{1,0:T(8,128)(2,1)} %qs_ref.1, bf16[128,128]{1,0:T(8,128)(2,1)} %ks_ref.1, bf16[128,128]{1,0:T(8,128)(2,1)} %vs_ref.1, bf16[128,128]{1,0:T(8,128)(2,1)} %ql_ref.1, bf16[128,128]{1,0:T(8,128)(2,1)} %kl_ref.1, bf16[128,128]{1,0:T(8,128)(2,1)} %vl_ref.1, ...), custom_call_target="tpu_custom_call" | custom-call | tf_op jit(solution)/shard_map/pallas_call | solution.py:642
  84.3 1.5 %copy.19 = bf16[16,2048]{1,0:T(8,128)(2,1)} copy(bf16[16,2048]{1,0:T(8,128)(2,1)} %shard_map.163) | data formatting | bytes 131072

commit v4 on v3

--- a/solution.py
+++ b/solution.py
@@ -35,6 +35,24 @@
     zn,
     yn,
     tn,
+    res_hbm,
+    qs_hbm,
+    ks_hbm,
+    vs_hbm,
+    ql_hbm,
+    kl_hbm,
+    vl_hbm,
+    fs_hbm,
+    fl_hbm,
+    wos_hbm,
+    wol_hbm,
+    gain_hbm,
+    wg_hbm,
+    wu_hbm,
+    cg_hbm,
+    cu_hbm,
+    wd_hbm,
+    out_ref,
     res_ref,
     qs_ref,
     ks_ref,
@@ -44,17 +62,14 @@
     vl_ref,
     fs_ref,
     fl_ref,
-    wos_hbm,
-    wol_hbm,
+    wos_ref,
+    wol_ref,
     gain_ref,
     wg_ref,
     wu_ref,
     cg_ref,
     cu_ref,
     wd_ref,
-    out_ref,
-    wos_ref,
-    wol_ref,
     gat,
     gatz,
     ty,
@@ -81,6 +96,8 @@
     fpi,
     dno,
     dni,
+    dnm,
+    dnx,
     first,
     ext,
     halo_out,
@@ -94,6 +111,8 @@
     t_r,
     w1_s,
     w1_r,
+    b_s,
+    b_r,
     w2_s,
     w2_r,
     o_s,
@@ -143,6 +162,29 @@
     def landed(dst, ss, rs):
         rc(dst, dst, ss, rs, yid(1)).wait_recv()
 
+    inputs = (
+        (res_hbm, res_ref),
+        (qs_hbm, qs_ref),
+        (ks_hbm, ks_ref),
+        (vs_hbm, vs_ref),
+        (ql_hbm, ql_ref),
+        (kl_hbm, kl_ref),
+        (vl_hbm, vl_ref),
+        (fs_hbm, fs_ref),
+        (fl_hbm, fl_ref),
+        (gain_hbm, gain_ref),
+        (wg_hbm, wg_ref),
+        (wu_hbm, wu_ref),
+        (cg_hbm, cg_ref),
+        (cu_hbm, cu_ref),
+        (wd_hbm, wd_ref),
+        (wos_hbm, wos_ref),
+        (wol_hbm, wol_ref),
+    )
+    loads = [pltpu.make_async_copy(a, b, loc_s.at[i]) for i, (a, b) in enumerate(inputs)]
+    for c in loads:
+        c.start()
+
     barrier = pltpu.get_barrier_semaphore()
     for i in range(1, yn):
         pl.semaphore_signal(barrier, inc=1, device_id=yid(i), device_id_type=MESH)
@@ -155,12 +197,8 @@
     def _():
         pl.semaphore_signal(barrier, inc=1, device_id=(sp - 1, tn - 1), device_id_type=MESH)
 
-    loads = [
-        pltpu.make_async_copy(wos_hbm, wos_ref, loc_s.at[0]),
-        pltpu.make_async_copy(wol_hbm, wol_ref, loc_s.at[1]),
-    ]
-    for c in loads:
-        c.start()
+    for c in loads[:-2]:
+        c.wait()
 
     def log_gate(x):
         u = jnp.exp(-jnp.abs(x))
@@ -242,10 +280,27 @@
         sl = w2_part(axis, o, s, way, part)
         landed(sl, w2_s.at[axis, k, part], w2_r.at[axis, k, part])
 
+    def hop(axis, g, start):
+        m, me, pos = (yn, z, y) if axis == 0 else (zn, y, z)
+        n = zn if axis == 0 else yn
+        b = lax.rem(pos + g + m, m)
+        for way in (0, 1):
+            o = me if start else lax.rem(me + (1 if way else -1) + n, n)
+            ref = wa.at[o, b] if axis == 0 else wb.at[b, o]
+            ss, rs = b_s.at[axis, way, g % m], b_r.at[axis, way, g % m]
+            if start:
+                send(ref, ref, ss, rs, (zid if axis == 0 else yid)(-1 if way else 1))
+            else:
+                landed(ref, ss, rs)
+
     def w2_step(s, part):
         for axis, n in ((0, zn), (1, yn)):
+            m = yn if axis == 0 else zn
+            if s == 2 and part == 0:
+                for g in range(m):
+                    hop(axis, g, False)
             for way in (0, 1):
-                if 1 < s <= n // 2 + 1:
+                if 2 < s <= n // 2 + 1:
                     w2_wait(axis, way, s - 1, part)
                 if s <= n // 2:
                     w2_send(axis, way, s, part)
@@ -254,6 +309,8 @@
         for axis in (0, 1):
             for way in (0, 1):
                 ring(axis, way, 1, kind, True)
+    hop(0, 0, True)
+    hop(1, 0, True)
 
     def ring_step(s, kinds):
         for kind in kinds:
@@ -283,6 +340,11 @@
             biass[h, i * tok : (i + 1) * tok] = column
     for s in range(2, max(hy, hz) + 1):
         ring_step(s, (0, 1, 2))
+        for axis, m in ((0, yn), (1, zn)):
+            if s == 2 and m > 2:
+                hop(axis, -1, True)
+            if s == 3 and m > 2:
+                hop(axis, 1, True)
         if s == 2:
             for i in range(1, zn):
                 landed(gatz.at[lax.rem(z - i + zn, zn)], gat_s.at[1, i], gat_r.at[1, i])
@@ -295,8 +357,10 @@
                     biasl[j, i * tok : (i + 1) * tok] = column
             edge[...] = -jnp.broadcast_to(gatz[z, 2:3], (tok, tok)).T
 
-    w2_step(1, 0)
-    w2_step(1, 1)
+    for axis, m in ((0, yn), (1, zn)):
+        for g in range(1, m):
+            if g not in (1, m - 1) or m == 2:
+                hop(axis, g, True)
     key_lane = lax.broadcasted_iota(jnp.int32, (tok, 128), 1)
     for i in range(yn):
         rows = slice(i * tok, (i + 1) * tok)
@@ -361,9 +425,6 @@
     def small_step(p, c):
         small(p, None)
         return c
-
-    lax.fori_loop(1, (zn - z + 1) // 2, small_step, 0)
-    small(0, y * tok + lax.broadcasted_iota(jnp.int32, (1, tok), 1))
 
     def large(p, c):
         a = lax.broadcasted_iota(jnp.int32, (tok, tok), 0)
@@ -402,6 +463,9 @@
         return c
 
     lax.fori_loop(0, yn // 2, large, 0)
+    lax.fori_loop(1, (zn - z + 1) // 2, small_step, 0)
+    small(0, y * tok + lax.broadcasted_iota(jnp.int32, (1, tok), 1))
+
     w2_step(2, 0)
     w2_step(2, 1)
 
@@ -448,7 +512,7 @@
         normed.append(att * lax.rsqrt(mean + EPS))
     nsm = jnp.concatenate(normed[:2], axis=0).T.astype(BF16)
     nla = normed[2].T.astype(BF16)
-    for c in loads:
+    for c in loads[-2:]:
         c.wait()
     width = min(512, d)
     for c in range(d // width):
@@ -522,14 +586,24 @@
             weight = w[c * zs : (c + 1) * zs, :, 2 * wrows : 3 * wrows].reshape(span, half)
             term = nt(hid[h], weight)
             total_down = term if total_down is None else total_down + term
-        dno[:, c * span : (c + 1) * span] = total_down.astype(BF16)
-    for i in range(1, tn):
-        send(mine(dno, lax.rem(tp + i, tn)), dni.at[i], d_s.at[i], d_r.at[i], tid(i))
-    value = first[...] + mine(dno, tp)[...].astype(F32)
-    for i in range(1, tn):
+        dno[:, :, :, c * span : (c + 1) * span] = total_down.astype(BF16).reshape(
+            tn // 2, 2, own, span
+        )
+    core = lax.rem(tp, 2)
+    mate = (sp, tp + 1 - 2 * core)
+    pairs = tn // 2
+    spot = tp // 2
+    send(dno.at[:, 1 - core], dnm, d_s.at[0], d_r.at[0], mate)
+    landed(dnm, d_s.at[0], d_r.at[0])
+    for i in range(1, pairs):
+        k = lax.rem(spot + i, pairs)
+        dnx[i] = (dno[k, core].astype(F32) + dnm[k].astype(F32)).astype(BF16)
+        send(dnx.at[i], dni.at[i], d_s.at[i], d_r.at[i], (sp, 2 * k + core))
+    value = first[...] + dno[spot, core].astype(F32) + dnm[spot].astype(F32)
+    for i in range(1, pairs):
         landed(dni.at[i], d_s.at[i], d_r.at[i])
         value = value + dni[i].astype(F32)
-    out_ref[...] = value.astype(BF16)
+    out_ref[...] = value
 
     for c in sends:
         c.wait_send()
@@ -578,11 +652,29 @@
     own, d = residual.shape
     wrows, ff = w_gate.shape
     half = ff // 2
+    operands = (
+        residual,
+        q_small,
+        k_small,
+        v_small,
+        q_large,
+        k_large,
+        v_large,
+        forget_small.T,
+        forget_large.T,
+        w_out_small,
+        w_out_large,
+        norm_gain.reshape(1, d),
+        w_gate,
+        w_up,
+        conv_gate,
+        conv_up,
+        w_down.T,
+    )
     dma = pltpu.SemaphoreType.DMA
     big = max(yn, zn)
     scratch = [
-        pltpu.VMEM(w_out_small.shape, BF16),
-        pltpu.VMEM(w_out_large.shape, BF16),
+        *(pltpu.VMEM(a.shape, a.dtype) for a in operands),
         pltpu.VMEM((yn, 8, tok), F32),
         pltpu.VMEM((zn, 16, tok), F32),
         pltpu.VMEM((yn, 3, tok, 128), BF16),
@@ -607,21 +699,25 @@
         pltpu.VMEM((2, big, 8, tok), F32),
         pltpu.VMEM((tok, d), BF16),
         pltpu.VMEM((tn, own, d), BF16),
-        pltpu.VMEM((tok, d), BF16),
-        pltpu.VMEM((tn, own, d), BF16),
+        pltpu.VMEM((tn // 2, 2, own, d), BF16),
+        pltpu.VMEM((tn // 2, own, d), BF16),
+        pltpu.VMEM((tn // 2, own, d), BF16),
+        pltpu.VMEM((tn // 2, own, d), BF16),
         pltpu.VMEM((own, d), F32),
         pltpu.VMEM((tok + 16, d), BF16),
         pltpu.VMEM((16, d // 8), BF16),
         pltpu.VMEM((16, d // 8), BF16),
         pltpu.VMEM((2, tok + 16, half), F32),
         pltpu.VMEM((2, tok, half), BF16),
-        dma((2,)),
+        dma((len(operands),)),
         dma((2, big)),
         dma((2, big)),
         dma((2, big, 2)),
         dma((2, big, 2)),
         dma((2, big)),
         dma((2, big)),
+        dma((2, 2, big)),
+        dma((2, 2, big)),
         dma((2, big, 2)),
         dma((2, big, 2)),
         dma((2, big)),
@@ -639,34 +735,17 @@
     ]
     vmem = pl.BlockSpec(memory_space=pltpu.VMEM)
     hbm = pl.BlockSpec(memory_space=pl.ANY)
-    return pl.pallas_call(
+    result = pl.pallas_call(
         functools.partial(kernel, zn, yn, tn),
-        out_shape=jax.ShapeDtypeStruct((own, d), BF16),
-        in_specs=[vmem] * 9 + [hbm] * 2 + [vmem] * 6,
+        out_shape=jax.ShapeDtypeStruct((own, d), F32),
+        in_specs=[hbm] * len(operands),
         out_specs=pl.BlockSpec(memory_space=pltpu.VMEM),
         scratch_shapes=scratch,
         compiler_params=pltpu.CompilerParams(
             collective_id=0, has_side_effects=True, vmem_limit_bytes=60 * 1024 * 1024
         ),
-    )(
-        residual,
-        q_small,
-        k_small,
-        v_small,
-        q_large,
-        k_large,
-        v_large,
-        forget_small.T,
-        forget_large.T,
-        w_out_small,
-        w_out_large,
-        norm_gain.reshape(1, d),
-        w_gate,
-        w_up,
-        conv_gate,
-        conv_up,
-        w_down.T,
-    )
+    )(*operands)
+    return result.astype(BF16)
 
 
 def solution(mesh):

time: 86 us -> 80.9 us (0.941)
  Pallas kernels: 84.3 us -> 79.2 us
  other arithmetic: 0 us -> 1.54 us
  local copies, waits for them, and re-layouts: 1.47 us -> 0 us
    pallas_call x1, Pallas kernels: 84.3 us -> 79.2 us  [body(): pl.pallas_call(functools.partial(kernel, zn, yn, tn), out_shape=jax.Shape...]
    convert_element_type x0 -> x1, other arithmetic: none -> 1.54 us  [body(): return result.astype(BF16)]
    unnamed x1 -> x0, local copies, waits for them, and re-layouts: 1.47 us -> none
where the time goes in v4:
time: 80.9 us; the launch traced here: 80.8 us
  Pallas kernels  79.2 us (98%)
  other arithmetic  1.54 us (2%)
    pallas_call x1, Pallas kernels, body(): pl.pallas_call(functools.partial(kernel, zn, yn, tn), out_shape=jax.Shape...  79.2 us

profile of v4, /device:TPU:1, one launch (start us, length us, event | category | flops | bytes accessed | tf_op | source)
XLA Modules:
  0.0 80.8 jit_solution(13005563201772966749)
XLA Ops:
  0.0 79.2 %shard_map.163 = f32[16,2048]{1,0:T(8,128)} custom-call(bf16[16,2048]{1,0:T(8,128)(2,1)} %res_hbm.1, bf16[128,128]{1,0:T(8,128)(2,1)} %qs_hbm.1, bf16[128,128]{1,0:T(8,128)(2,1)} %ks_hbm.1, bf16[128,128]{1,0:T(8,128)(2,1)} %vs_hbm.1, bf16[128,128]{1,0:T(8,128)(2,1)} %ql_hbm.1, bf16[128,128]{1,0:T(8,128)(2,1)} %kl_hbm.1, bf16[128,128]{1,0:T(8,128)(2,1)} %vl_hbm.1, ...), custom_call_target="tpu_custom_call" | custom-call | tf_op jit(solution)/shard_map/pallas_call | solution.py:738
  79.2 1.5 %convert_element_type.3 = bf16[16,2048]{1,0:T(8,128)(2,1)} convert(f32[16,2048]{1,0:T(8,128)} %shard_map.163) | non-fusion elementwise | flops 32768 | bytes 196608 | tf_op jit(solution)/shard_map/convert_element_type | solution.py:748

commit v5 on v4

--- a/solution.py
+++ b/solution.py
@@ -262,7 +262,8 @@
         if s < n // 2:
             span = pl.ds(0, m)
         else:
-            span = pl.ds(way * (m // 2), m // 2)
+            cut = max(1, 2 * m // 8)
+            span = pl.ds(cut, m - cut) if way else pl.ds(0, cut)
         return wa.at[o, span, rows] if axis == 0 else wb.at[span, o, rows]
 
     def w2_send(axis, way, s, part):
@@ -345,6 +346,7 @@
                 hop(axis, -1, True)
             if s == 3 and m > 2:
                 hop(axis, 1, True)
+                hop(axis, -2, True)
         if s == 2:
             for i in range(1, zn):
                 landed(gatz.at[lax.rem(z - i + zn, zn)], gat_s.at[1, i], gat_r.at[1, i])
@@ -359,7 +361,7 @@
 
     for axis, m in ((0, yn), (1, zn)):
         for g in range(1, m):
-            if g not in (1, m - 1) or m == 2:
+            if g not in (1, m - 1, m - 2):
                 hop(axis, g, True)
     key_lane = lax.broadcasted_iota(jnp.int32, (tok, 128), 1)
     for i in range(yn):
@@ -737,7 +739,7 @@
     hbm = pl.BlockSpec(memory_space=pl.ANY)
     result = pl.pallas_call(
         functools.partial(kernel, zn, yn, tn),
-        out_shape=jax.ShapeDtypeStruct((own, d), F32),
+        out_shape=pltpu.VMEM((own, d), F32),
         in_specs=[hbm] * len(operands),
         out_specs=pl.BlockSpec(memory_space=pltpu.VMEM),
         scratch_shapes=scratch,

time: 80.9 us -> 79.3 us (0.980)
  other arithmetic: 1.54 us -> 0.64 us
    convert_element_type x1, other arithmetic: 1.54 us -> 0.64 us  [body(): return result.astype(BF16)]
where the time goes in v5:
time: 79.3 us; the launch traced here: 79.2 us
  Pallas kernels  78.5 us (99%)
    pallas_call x1, Pallas kernels, body(): pl.pallas_call(functools.partial(kernel, zn, yn, tn), out_shape=pltpu.VME...  78.5 us

profile of v5, /device:TPU:1, one launch (start us, length us, event | category | flops | bytes accessed | tf_op | source)
XLA Modules:
  0.0 79.2 jit_solution(1873387644116308632)
XLA Ops:
  0.0 78.5 %shard_map.163 = f32[16,2048]{1,0:T(8,128)S(1)} custom-call(bf16[16,2048]{1,0:T(8,128)(2,1)} %res_hbm.1, bf16[128,128]{1,0:T(8,128)(2,1)} %qs_hbm.1, bf16[128,128]{1,0:T(8,128)(2,1)} %ks_hbm.1, bf16[128,128]{1,0:T(8,128)(2,1)} %vs_hbm.1, bf16[128,128]{1,0:T(8,128)(2,1)} %ql_hbm.1, bf16[128,128]{1,0:T(8,128)(2,1)} %kl_hbm.1, bf16[128,128]{1,0:T(8,128)(2,1)} %vl_hbm.1, ...), custom_call_target="tpu_custom_call" | custom-call | tf_op jit(solution)/shard_map/pallas_call | solution.py:740
  78.5 0.6 convert_element_type.3
